TPU v7x, 128 devices: a whole 4x4x4 slice. The times are simulated.
128 devices in a mesh: sp: 32 (over z, y, core), tp: 4 (over x).
Axes of the slice: x: 4, y: 4, z: 4, core: 2. Of those that a mesh axis runs over, the one named last changes fastest.
Arguments:
- query_rows: bfloat16 [32768, 1024], P('sp', 'tp'), may hold values from -6 to 6
- key_rows: bfloat16 [32768, 1024], P('sp', 'tp'), may hold values from -6 to 6
- value_rows: bfloat16 [32768, 1024], P('sp', 'tp'), may hold values from -6 to 6
- input_gate: float32 [8, 32768], P('tp', 'sp'), may hold values from -4 to 255
- forget_gate: float32 [8, 32768], P('tp', 'sp'), may hold values from -3 to 20
- output_gate: bfloat16 [32768, 1024], P('sp', 'tp'), may hold values from -6 to 6
- documents: int32 [32768], P('sp'), may hold values from 0 to 7, never falling along the last dimension, each value on 1 to 6144 neighbouring positions
- residual: bfloat16 [32768, 2048], P(('sp', 'tp')), may hold values from -6 to 6
- out_weight: bfloat16 [1024, 2048], P('tp'), may hold values from -0.375 to 0.375
- norm_gain: bfloat16 [2048], replicated, may hold values from 0.099609375 to 1.8984375
- gate_weight: bfloat16 [2048, 5632], P('sp', 'tp'), may hold values from -0.125 to 0.125
- up_weight: bfloat16 [2048, 5632], P('sp', 'tp'), may hold values from -0.125 to 0.125
- down_weight: bfloat16 [5632, 2048], P('tp', 'sp'), may hold values from -0.15625 to 0.15625
Outputs:
- layer_out: bfloat16 [32768, 2048], P(('sp', 'tp'))
Inputs may be any that keep to these rules, and one draw needn't show every extreme that they name: `documents`: document numbers never fall along the positions; each document covers 1 to 6144 positions and one covers exactly 6144.
All inputs are finite; a program needn't handle non-finite values.
Results may differ from a plain program's by a relative error of at most 0.013.
Values may be sent and summed in bfloat16 or wider, within the bound.
A program may use at most 128 MiB of HBM per device.

v0:
```python
import jax
import jax.numpy as jnp
from jax import lax
from jax.sharding import Mesh
from jax.sharding import PartitionSpec as P

HD = 128
BLOCK = 128
SP = ("sp_0", "sp_1", "sp_2")
SP_TP = ("sp_0", "sp_1", "sp_2", "tp")


neg_large = -1e30
norm_eps = 1e-06
highest = lax.Precision.HIGHEST


def gather_turned(arrays, axis, dims):
    turned = [jnp.moveaxis(a, dim, 0) for a, dim in zip(arrays, dims)]
    both = jnp.concatenate([t.reshape(len(t), -1) for t in turned], axis=1)
    whole, at, finished = (lax.all_gather(both, axis, axis=0, tiled=True), 0, [])
    for t, dim in zip(turned, dims):
        slab = whole[:, at : at + t[0].size].reshape(-1, *t.shape[1:])
        finished.append(jnp.moveaxis(slab, 0, dim))
        at += t[0].size
    return tuple(finished)


def nothing_yet(array, identity):
    return jax.tree.map(
        lambda part, zero: jnp.zeros_like(part) + jnp.asarray(zero, part.dtype), array, identity
    )


def all_in_one(array, axis):
    leaves = jax.tree.leaves(array)
    sequence = sorted(range(len(leaves)), key=lambda k: -leaves[k].size)
    width = (1, *leaves[sequence[0]].shape)[-1]
    lines = [
        jnp.pad(leaves[k].reshape(-1), (0, -leaves[k].size % width)).reshape(-1, width)
        for k in sequence
    ]
    both, at, found = (lax.all_gather(jnp.concatenate(lines), axis), 0, {})
    for k, line in zip(sequence, lines):
        slab = both[:, at : at + len(line)].reshape(len(both), -1)
        found[k] = slab[:, : leaves[k].size].reshape(-1, *leaves[k].shape)
        at += len(line)
    numbers = iter(range(len(leaves)))
    return jax.tree.map(lambda _: found[next(numbers)], array)


def gathered_by_type(array, axis):
    leaves, found = (jax.tree.leaves(array), {})
    for leading, a in enumerate(leaves):
        if leading not in found:
            alike = [k for k, b in enumerate(leaves) if b.dtype == a.dtype]
            got = (
                all_in_one([leaves[k] for k in alike], axis)
                if len(alike) > 1
                else [lax.all_gather(a, axis)]
            )
            for k, b in zip(alike, got):
                found[k] = b
    numbers = iter(range(len(leaves)))
    return jax.tree.map(lambda _: found[next(numbers)], array)


def prefix_by_axis(array, axes, combine, identity):
    before = start = nothing_yet(array, identity)
    total = array
    for axis in reversed(axes):
        devices, position = (lax.axis_size(axis), lax.axis_index(axis))
        pieces = gathered_by_type(total, axis)
        inside, total = (start, start)
        for k in range(devices):
            passed = k < position
            total = combine(total, jax.tree.map(lambda part: part[k], pieces))
            inside = jax.tree.map(lambda new, old: jnp.where(passed, new, old), total, inside)
        before = combine(inside, before)
    return before


def block_step(carried, inputs):
    memory, normer, stab_prev, carry_doc = carried
    queries, key_float, value_float, gate_in, log_forget, docs = inputs
    cumlog = jnp.cumsum(log_forget, axis=1)
    length = docs.shape[0]
    target_positions = jnp.arange(length)
    same_doc = (docs[:, None] == docs[None, :]) & (
        target_positions[:, None] >= target_positions[None, :]
    )
    log_weight = jnp.where(
        same_doc[None], cumlog[:, :, None] - cumlog[:, None, :] + gate_in[:, None, :], neg_large
    )
    carried_log = jnp.where((docs == carry_doc)[None, :], cumlog + stab_prev[:, None], neg_large)
    stabilizer = jnp.maximum(carried_log, jnp.max(log_weight, axis=2))
    scores = jnp.einsum("lhd,shd->hls", queries, key_float, precision=highest)
    weighted = scores * jnp.exp(log_weight - stabilizer[:, :, None])
    carried_scale = jnp.exp(carried_log - stabilizer)
    numerator = carried_scale[:, :, None] * jnp.einsum(
        "lhd,hde->hle", queries, memory, precision=highest
    )
    numerator = numerator + jnp.einsum("hls,she->hle", weighted, value_float, precision=highest)
    denominator = carried_scale * jnp.einsum(
        "lhd,hd->hl", queries, normer, precision=highest
    ) + jnp.sum(weighted, axis=2)
    outputs = numerator / jnp.maximum(jnp.abs(denominator), 1.0)[:, :, None]
    last_doc = docs[-1]
    inject_log = jnp.where(
        (docs == last_doc)[None, :], cumlog[:, -1:] - cumlog + gate_in, neg_large
    )
    inject_max = jnp.max(inject_log, axis=1)
    weights = jnp.exp(inject_log - inject_max[:, None])
    continues = carry_doc == last_doc
    stab_new = jnp.where(continues, jnp.maximum(cumlog[:, -1] + stab_prev, inject_max), inject_max)
    decay_scale = jnp.where(continues, jnp.exp(cumlog[:, -1] + stab_prev - stab_new), 0.0)
    inject = jnp.exp(inject_max - stab_new)
    memory_step = jnp.einsum(
        "lhd,lhe->hde", key_float * weights.T[:, :, None], value_float, precision=highest
    )
    normer_step = jnp.einsum("hl,lhd->hd", weights, key_float, precision=highest)
    memory = decay_scale[:, None, None] * memory + inject[:, None, None] * memory_step
    normer = decay_scale[:, None] * normer + inject[:, None] * normer_step
    return ((memory, normer, stab_new, last_doc), jnp.transpose(outputs, (1, 0, 2)))


def run_blocks(queries, key_float, value_float, gate_in, log_forget, docs, start_state):
    length, heads, width = queries.shape
    count = length // BLOCK
    inputs = (
        queries.reshape(count, BLOCK, heads, width),
        key_float.reshape(count, BLOCK, heads, width),
        value_float.reshape(count, BLOCK, heads, width),
        jnp.moveaxis(gate_in.reshape(heads, count, BLOCK), 1, 0),
        jnp.moveaxis(log_forget.reshape(heads, count, BLOCK), 1, 0),
        docs.reshape(count, BLOCK),
    )
    final, outputs = lax.scan(block_step, start_state, inputs)
    return (outputs.reshape(length, heads, width), final)


def join_states(earlier, later_part):
    memory_early, normer_early, stab_early, total_early, doc_early = earlier
    memory_late, normer_late, stab_late, total_late, doc_late = later_part
    continues = doc_late == doc_early
    is_empty = doc_late < 0
    stab_both = jnp.where(continues, jnp.maximum(total_late + stab_early, stab_late), stab_late)
    scale_early = jnp.where(continues, jnp.exp(total_late + stab_early - stab_both), 0.0)
    scale_late = jnp.exp(stab_late - stab_both)
    memory = scale_early[:, None, None] * memory_early + scale_late[:, None, None] * memory_late
    normer = scale_early[:, None] * normer_early + scale_late[:, None] * normer_late
    return (
        jnp.where(is_empty, memory_early, memory),
        jnp.where(is_empty, normer_early, normer),
        jnp.where(is_empty, stab_early, stab_both),
        total_early + total_late,
        jnp.where(is_empty, doc_early, doc_late),
    )


def body(
    query_rows,
    key_rows,
    value_rows,
    input_gate,
    forget_gate,
    output_gate,
    documents,
    residual,
    out_weight,
    norm_gain,
    gate_weight,
    up_weight,
    down_weight,
):
    whole_gate, whole_up, whole_down = gather_turned(
        (gate_weight, up_weight, down_weight), SP, (0, 0, 1)
    )
    tokens = query_rows.shape[0]
    local_heads = input_gate.shape[0]
    queries = query_rows.astype(jnp.float32).reshape(tokens, local_heads, HD) * HD ** (-0.5)
    key_float = key_rows.astype(jnp.float32).reshape(tokens, local_heads, HD)
    value_float = value_rows.astype(jnp.float32).reshape(tokens, local_heads, HD)
    log_forget = jax.nn.log_sigmoid(forget_gate)
    cumlog = jnp.cumsum(log_forget, axis=1)
    total = cumlog[:, -1]
    last_doc = documents[-1]
    inject_log = jnp.where(
        (documents == last_doc)[None, :], total[:, None] - cumlog + input_gate, neg_large
    )
    inject_max = jnp.max(inject_log, axis=1)
    weights = jnp.exp(inject_log - inject_max[:, None])
    memory = jnp.einsum(
        "thd,the->hde", key_float * weights.T[:, :, None], value_float, precision=highest
    )
    normer = jnp.einsum("ht,thd->hd", weights, key_float, precision=highest)
    identity = (
        jnp.zeros_like(memory),
        jnp.zeros_like(normer),
        jnp.full_like(inject_max, neg_large),
        jnp.zeros_like(total),
        jnp.array(-1, jnp.int32),
    )
    before = prefix_by_axis(
        (memory, normer, inject_max, total, last_doc), SP, join_states, identity
    )
    cells, final = run_blocks(
        queries,
        key_float,
        value_float,
        input_gate,
        log_forget,
        documents,
        (before[0], before[1], before[2], before[4]),
    )
    gated = (cells.reshape(tokens, -1) * jax.nn.sigmoid(output_gate.astype(jnp.float32))).astype(
        jnp.bfloat16
    )
    mine = lax.all_to_all(gated, "tp", split_axis=0, concat_axis=1, tiled=True)
    projected = jnp.dot(
        mine,
        lax.all_gather(out_weight, "tp", axis=0, tiled=True),
        preferred_element_type=jnp.float32,
    )
    stream = residual.astype(jnp.float32) + projected
    normed = stream * lax.rsqrt(jnp.mean(stream * stream, axis=1, keepdims=True) + norm_eps)
    normed = (normed * norm_gain.astype(jnp.float32)).astype(jnp.bfloat16)
    rows_all = lax.all_gather(normed, "tp", axis=0, tiled=True)
    gate_act = jnp.dot(rows_all, whole_gate, preferred_element_type=jnp.float32)
    up_act = jnp.dot(rows_all, whole_up, preferred_element_type=jnp.float32)
    hidden = (jax.nn.silu(gate_act) * up_act).astype(jnp.bfloat16)
    partial_sum = jnp.dot(hidden, whole_down, preferred_element_type=jnp.float32)
    down = lax.psum_scatter(
        partial_sum.astype(jnp.bfloat16), "tp", scatter_dimension=0, tiled=True
    ).astype(jnp.float32)
    return (stream + 0.5 * down).astype(jnp.bfloat16)


def solution(mesh):
    torus = Mesh(mesh.devices.reshape(4, 4, 2, mesh.shape["tp"]), ("sp_0", "sp_1", "sp_2", "tp"))
    in_specs = (
        P(SP, "tp"),
        P(SP, "tp"),
        P(SP, "tp"),
        P("tp", SP),
        P("tp", SP),
        P(SP, "tp"),
        P(SP),
        P(SP_TP, None),
        P("tp", None),
        P(),
        P(SP, "tp"),
        P(SP, "tp"),
        P("tp", SP),
    )
    out_specs = P(SP_TP, None)
    return jax.shard_map(body, mesh=torus, in_specs=in_specs, out_specs=out_specs, check_vma=False)
```

profile of v0, /device:TPU:1, one launch (start us, length us, event | category | flops | bytes accessed | tf_op | source)
XLA Modules:
  0.0 448.9 jit_solution(14347902271754953552)
XLA Ops:
  10.0 1.9 slice_dynamic-update-slice_fusion
  19.8 3.2 all-gather.3
  31.0 11.8 %all-gather.4 = f32[4,260,128]{2,1,0:T(8,128)S(1)} all-gather(f32[1,260,128]{2,1,0:T(8,128)S(1)} %maximum_bitcast_fusion.1), channel_id=3, replica_groups=mesh['sp_0'=4,'sp_1'=4,'sp_2'=2,'tp'=4] {'sp_1'}, dimensions={0}, use_global_device_ids=true | all-gather | bytes 665600 | tf_op jit(solution)/shard_map/all_gather | solution.py:43
  45.5 6.5 %all-reduce.7 = s32[4]{0:T(128)S(1)} all-reduce(s32[4]{0:T(128)S(1)} %dynamic-update-slice.1), channel_id=1, replica_groups=mesh['sp_0'=4,'sp_1'=4,'sp_2'=2,'tp'=4] {'sp_1'}, use_global_device_ids=true, to_apply=%add.7 | all-reduce | flops 4 | bytes 32
  61.6 11.7 %all-gather.5 = f32[4,260,128]{2,1,0:T(8,128)S(1)} all-gather(f32[1,260,128]{2,1,0:T(8,128)S(1)} %maximum_bitcast_fusion.2), channel_id=4, replica_groups=mesh['sp_0'=4,'sp_1'=4,'sp_2'=2,'tp'=4] {'sp_0'}, dimensions={0}, use_global_device_ids=true | all-gather | bytes 665600 | tf_op jit(solution)/shard_map/all_gather | solution.py:43
  77.6 7.2 %all-reduce.8 = s32[4]{0:T(128)S(1)} all-reduce(s32[4]{0:T(128)S(1)} %dynamic-update-slice.2), channel_id=1, replica_groups=mesh['sp_0'=4,'sp_1'=4,'sp_2'=2,'tp'=4] {'sp_0'}, use_global_device_ids=true, to_apply=%add.8 | all-reduce | flops 4 | bytes 32
  97.7 112.4 %while.18 = (s32[]{:T(128)}, f32[2,128,128]{2,1,0:T(8,128)S(1)}, f32[2,128]{1,0:T(2,128)S(1)}, f32[2]{0:T(128)S(1)}, s32[]{:T(128)}, /*index=5*/f32[8,128,2,128]...) while((s32[]{:T(128)}, f32[2,128,128]{2,1,0:T(8,128)S(1)}, ...), condition=%wide.region_8.9_spmd, body=%wide.region_3.8_spmd.sunk | while | flops 202756624 | bytes 3499011 | solution.py:138
  106.4 4.7 %dynamic_update_slice.5 = f32[8,128,2,128]{1,0,3,2:T(8,128)} dynamic-update-slice(f32[8,128,2,128]{1,0,3,2:T(8,128)} %get-tuple-element.360, f32[1,128,2,128]{1,0,3,2:T(1,128)S(1)} %copy.134, s32[]{:T(128)S(6)} %copy.145, s32[]{:T(128)} %constant.31.clone.1..sunk, s32[]{:T(128)} %constant.31.clone.1..sunk, s32[]{:T(128)} %constant.31.clone.1..sunk) | dynamic-update-slice | bytes 262148 | tf_op jit(solution)/shard_map/while/body/jit(dynamic_update_index_in_dim)/dynamic_update_slice | solution.py:138
  120.5 4.7 %dynamic_update_slice.5 = f32[8,128,2,128]{1,0,3,2:T(8,128)} dynamic-update-slice(f32[8,128,2,128]{1,0,3,2:T(8,128)} %get-tuple-element.360, f32[1,128,2,128]{1,0,3,2:T(1,128)S(1)} %copy.134, s32[]{:T(128)S(6)} %copy.145, s32[]{:T(128)} %constant.31.clone.1..sunk, s32[]{:T(128)} %constant.31.clone.1..sunk, s32[]{:T(128)} %constant.31.clone.1..sunk) | dynamic-update-slice | bytes 262148 | tf_op jit(solution)/shard_map/while/body/jit(dynamic_update_index_in_dim)/dynamic_update_slice | solution.py:138
  134.5 4.7 %dynamic_update_slice.5 = f32[8,128,2,128]{1,0,3,2:T(8,128)} dynamic-update-slice(f32[8,128,2,128]{1,0,3,2:T(8,128)} %get-tuple-element.360, f32[1,128,2,128]{1,0,3,2:T(1,128)S(1)} %copy.134, s32[]{:T(128)S(6)} %copy.145, s32[]{:T(128)} %constant.31.clone.1..sunk, s32[]{:T(128)} %constant.31.clone.1..sunk, s32[]{:T(128)} %constant.31.clone.1..sunk) | dynamic-update-slice | bytes 262148 | tf_op jit(solution)/shard_map/while/body/jit(dynamic_update_index_in_dim)/dynamic_update_slice | solution.py:138
  148.6 4.7 %dynamic_update_slice.5 = f32[8,128,2,128]{1,0,3,2:T(8,128)} dynamic-update-slice(f32[8,128,2,128]{1,0,3,2:T(8,128)} %get-tuple-element.360, f32[1,128,2,128]{1,0,3,2:T(1,128)S(1)} %copy.134, s32[]{:T(128)S(6)} %copy.145, s32[]{:T(128)} %constant.31.clone.1..sunk, s32[]{:T(128)} %constant.31.clone.1..sunk, s32[]{:T(128)} %constant.31.clone.1..sunk) | dynamic-update-slice | bytes 262148 | tf_op jit(solution)/shard_map/while/body/jit(dynamic_update_index_in_dim)/dynamic_update_slice | solution.py:138
  162.6 4.7 %dynamic_update_slice.5 = f32[8,128,2,128]{1,0,3,2:T(8,128)} dynamic-update-slice(f32[8,128,2,128]{1,0,3,2:T(8,128)} %get-tuple-element.360, f32[1,128,2,128]{1,0,3,2:T(1,128)S(1)} %copy.134, s32[]{:T(128)S(6)} %copy.145, s32[]{:T(128)} %constant.31.clone.1..sunk, s32[]{:T(128)} %constant.31.clone.1..sunk, s32[]{:T(128)} %constant.31.clone.1..sunk) | dynamic-update-slice | bytes 262148 | tf_op jit(solution)/shard_map/while/body/jit(dynamic_update_index_in_dim)/dynamic_update_slice | solution.py:138
  176.6 4.7 %dynamic_update_slice.5 = f32[8,128,2,128]{1,0,3,2:T(8,128)} dynamic-update-slice(f32[8,128,2,128]{1,0,3,2:T(8,128)} %get-tuple-element.360, f32[1,128,2,128]{1,0,3,2:T(1,128)S(1)} %copy.134, s32[]{:T(128)S(6)} %copy.145, s32[]{:T(128)} %constant.31.clone.1..sunk, s32[]{:T(128)} %constant.31.clone.1..sunk, s32[]{:T(128)} %constant.31.clone.1..sunk) | dynamic-update-slice | bytes 262148 | tf_op jit(solution)/shard_map/while/body/jit(dynamic_update_index_in_dim)/dynamic_update_slice | solution.py:138
  190.7 4.7 %dynamic_update_slice.5 = f32[8,128,2,128]{1,0,3,2:T(8,128)} dynamic-update-slice(f32[8,128,2,128]{1,0,3,2:T(8,128)} %get-tuple-element.360, f32[1,128,2,128]{1,0,3,2:T(1,128)S(1)} %copy.134, s32[]{:T(128)S(6)} %copy.145, s32[]{:T(128)} %constant.31.clone.1..sunk, s32[]{:T(128)} %constant.31.clone.1..sunk, s32[]{:T(128)} %constant.31.clone.1..sunk) | dynamic-update-slice | bytes 262148 | tf_op jit(solution)/shard_map/while/body/jit(dynamic_update_index_in_dim)/dynamic_update_slice | solution.py:138
  204.7 4.7 %dynamic_update_slice.5 = f32[8,128,2,128]{1,0,3,2:T(8,128)} dynamic-update-slice(f32[8,128,2,128]{1,0,3,2:T(8,128)} %get-tuple-element.360, f32[1,128,2,128]{1,0,3,2:T(1,128)S(1)} %copy.134, s32[]{:T(128)S(6)} %copy.145, s32[]{:T(128)} %constant.31.clone.1..sunk, s32[]{:T(128)} %constant.31.clone.1..sunk, s32[]{:T(128)} %constant.31.clone.1..sunk) | dynamic-update-slice | bytes 262148 | tf_op jit(solution)/shard_map/while/body/jit(dynamic_update_index_in_dim)/dynamic_update_slice | solution.py:138
  212.8 3.7 all-to-all-start
  216.5 6.9 %all-to-all-done = bf16[4,256,256]{1,2,0:T(8,128)(2,1)S(1)} async-done(((bf16[4,256,256]{1,2,0:T(8,128)(2,1)}), bf16[4,256,256]{1,2,0:T(8,128)(2,1)S(1)}, u32[]{:S(2)}, u32[]{:S(2)}) %all-to-all-start) | async-done | bytes 524320 | tf_op jit(solution)/shard_map/all_to_all | solution.py:219
  223.4 3.9 multiply_reduce_fusion
  229.8 52.7 %all-gather.12.cloned.1.call-done = bf16[1024,2048]{1,0:T(8,128)(2,1)} async-done(((bf16[256,2048]{1,0:T(8,128)(2,1)}), bf16[1024,2048]{1,0:T(8,128)(2,1)}) %all-gather.12.cloned.1.call-update) | async-done | bytes 4194320 | tf_op jit(solution)/shard_map/all_gather | solution.py:228
  282.5 77.2 %all-gather.14.cloned.1.call-done = bf16[2048,4224]{1,0:T(8,128)(2,1)} async-done(((bf16[64,4224]{1,0:T(8,128)(2,1)}), bf16[2048,4224]{1,0:T(8,128)(2,1)}) %all-gather.14.cloned.1.call-update) | async-done | bytes 17301520 | tf_op jit(solution)/shard_map/all_gather | solution.py:21
  359.6 11.7 %fusion.21 = f32[1024,1408]{1,0:T(8,128)} fusion(bf16[1024,2048]{1,0:T(8,128)(2,1)} %all-gather.12.cloned.1.call-done, bf16[2048,4224]{1,0:T(8,128)(2,1)} %all-gather.14.cloned.1.call-done), kind=kOutput, calls=%fused_computation.48 | convolution fusion | flops 5905580032 | bytes 15728640 | tf_op jit(solution)/shard_map/dot_general | solution.py:229
  371.3 22.7 %fusion.25 = bf16[1024,2048]{1,0:T(8,128)(2,1)} fusion(bf16[2048,4224]{1,0:T(8,128)(2,1)} %all-gather.14.cloned.1.call-done, f32[1024,1408]{1,0:T(8,128)} %fusion.21, bf16[1024,2048]{1,0:T(8,128)(2,1)} %all-gather.12.cloned.1.call-done), kind=kOutput, calls=%fused_computation.51 | convolution fusion | flops 11821907968 | bytes 25690112 | tf_op jit(solution)/shard_map/dot_general | solution.py:232
  394.0 45.9 %reduce-scatter.2.cloned.1.call-done = bf16[256,2048]{1,0:T(8,128)(2,1)} async-done(((bf16[1024,2048]{1,0:T(8,128)(2,1)}), bf16[256,2048]{1,0:T(8,128)(2,1)}) %reduce-scatter.2.cloned.1.call-update) | async-done | bytes 1048592 | tf_op jit(solution)/shard_map/reduce_scatter | solution.py:233
  439.9 2.5 add_convert_fusion
  (303 shorter events, 97.9 us)
Async XLA Ops:
  6.5 37.1 %copy-start.9 = (u32[128]{0:T(128)S(1)}, u32[128]{0:T(128)}, u32[]{:S(2)}) copy-start(u32[128]{0:T(128)} %constant.104) | copy-start | bytes 1540
  6.5 38.5 %copy-start.1 = (bf16[1024,256]{1,0:T(8,128)(2,1)S(1)}, bf16[1024,256]{1,0:T(8,128)(2,1)}, u32[]{:S(2)}) copy-start(bf16[1024,256]{1,0:T(8,128)(2,1)} %param.17) | copy-start | bytes 1572868
  6.5 216.9 %all-gather.10.cloned.1.call-start = ((), (), s32[]{:S(2)}) async-start(), calls=%async_computation.2 | async-start | bytes 5242880 | tf_op jit(solution)/shard_map/all_gather | solution.py:222
  19.7 54.4 %copy-start = (bf16[1024,256]{1,0:T(8,128)(2,1)S(1)}, bf16[1024,256]{1,0:T(8,128)(2,1)}, u32[]{:S(2)}) copy-start(bf16[1024,256]{1,0:T(8,128)(2,1)} %param.16) | copy-start | bytes 1572868
  30.2 0.5 copy-start.7
  60.6 0.6 copy-start.8
  97.7 112.4 %copy-start.2 = (bf16[1024,256]{1,0:T(8,128)(2,1)S(1)}, bf16[1024,256]{1,0:T(8,128)(2,1)}, u32[]{:S(2)}) copy-start(bf16[1024,256]{1,0:T(8,128)(2,1)} %param.20) | copy-start | bytes 1572868
  210.1 6.4 %copy-start.6 = (bf16[2048]{0:T(1024)(128)(2,1)S(1)}, bf16[2048]{0:T(1024)(128)(2,1)}, u32[]{:S(2)}) copy-start(bf16[2048]{0:T(1024)(128)(2,1)} %param.24) | copy-start | bytes 12292
  212.8 10.7 %all-to-all-start = ((bf16[4,256,256]{1,2,0:T(8,128)(2,1)}), bf16[4,256,256]{1,2,0:T(8,128)(2,1)S(1)}, u32[]{:S(2)}, u32[]{:S(2)}) async-start(bf16[4,256,256]{1,2,0:T(8,128)(2,1)} %bitcast.516), calls=%async_computation | async-start | bytes 1048576 | tf_op jit(solution)/shard_map/all_to_all | solution.py:219
  216.5 66.0 %all-gather.12.cloned.1.call-start = ((), (), s32[]{:S(2)}) async-start(), calls=%async_computation.3 | async-start | bytes 5242880 | tf_op jit(solution)/shard_map/all_gather | solution.py:228
  227.3 1.3 copy-start.3
  227.3 1.3 copy-start.4
  227.3 1.3 copy-start.5
  228.6 131.1 %all-gather.14.cloned.1.call-start = ((), (), s32[]{:S(2)}) async-start(), calls=%async_computation.4 | async-start | bytes 17842176 | tf_op jit(solution)/shard_map/all_gather | solution.py:21
  229.5 210.4 %reduce-scatter.2.cloned.1.call-start = ((), (), s32[]{:S(2)}) async-start(), calls=%async_computation.5 | async-start | bytes 5242880 | tf_op jit(solution)/shard_map/reduce_scatter | solution.py:233
Sparse Core Ops, SparseCore 0:
  9.0 51.1 all-gather.9
  228.7 53.7 all-gather.11
  284.7 74.8 all-gather.13
  394.2 45.7 reduce-scatter.1
where the time goes:
time: 451 us; the launch traced here: 449 us
  waiting for transfers between devices  183 us (41%)
  local copies, waits for them, and re-layouts  78.3 us (17%)
  matrix products  58.1 us (13%)
  blocking collectives  42.2 us (9%)
  other arithmetic  39.2 us (9%)
  between operations  32.8 us (7%)
  loops' own time  10.8 us (2%)
    all_gather x1, waiting for transfers between devices, gather_turned(): lax.all_gather(both, axis, axis=0, tiled=True)  77.2 us
    all_gather x1, waiting for transfers between devices, body(): rows_all = lax.all_gather(normed, 'tp', axis=0, tiled=True)  52.7 us
    reduce_scatter x1, waiting for transfers between devices, body(): lax.psum_scatter(partial_sum.astype(jnp.bfloat16), 'tp', scatter_dimensio...  45.9 us
    dynamic_update_slice x16, local copies, waits for them, and re-layouts, run_blocks(): final, outputs = lax.scan(block_step, start_state, inputs)  38.7 us
    all_gather x3, blocking collectives, all_in_one(): both, at, found = (lax.all_gather(jnp.concatenate(lines), axis), 0, {})  26.6 us
    dot_general x1, matrix products, body(): jnp.dot(hidden, whole_down, preferred_element_type=jnp.float32)  22.7 us
    unnamed x3, blocking collectives  15.6 us
    dynamic_slice x16, local copies, waits for them, and re-layouts, run_blocks(): final, outputs = lax.scan(block_step, start_state, inputs)  14.8 us
  transfers between devices with their start and end apart: 5, of which 4 were waited for; matrix products, arithmetic and copies ran while one was open for 30% of the time, Pallas kernels for 0%

commit v1 on v0

v1 whole, which is shorter than its diff:
```python
import jax
import jax.numpy as jnp
from jax import lax
from jax.experimental import pallas as pl
from jax.experimental.pallas import tpu as pltpu
from jax.sharding import Mesh
from jax.sharding import PartitionSpec as P

HD = 128
SP = ("sp_0", "sp_1", "sp_2")
SP_TP = ("sp_0", "sp_1", "sp_2", "tp")
MESH = pl.DeviceIdType.MESH
BF = jnp.bfloat16
F32 = jnp.float32

NORM_EPS = 1e-06
NEG = -1e30
T = 1024
R = 256
D = 2048
FD = 1408
NJ = FD // 128
LOOK = 6
TILES = 3 * NJ
PARTS = ((0, 16, 8), (16, 17, 9))


def dot(a, b):
    return jnp.dot(a, b, preferred_element_type=F32)


def dot_nt(a, b):
    return lax.dot_general(a, b, (((1,), (1,)), ((), ())), preferred_element_type=F32)


def dot_tn(a, b):
    return lax.dot_general(a, b, (((0,), (0,)), ((), ())), preferred_element_type=F32)


def split(a):
    hi = a.astype(BF)
    return hi, (a - hi.astype(F32)).astype(BF)


def kernel(
    gates,
    gain,
    q_hbm,
    k_hbm,
    v_hbm,
    og_hbm,
    res_hbm,
    ow_hbm,
    wg_hbm,
    wu_hbm,
    wd_hbm,
    out,
    q,
    k,
    v,
    og,
    res,
    wg,
    wu,
    wd,
    w,
    ow,
    st_out,
    st_in,
    gate_out,
    gate_in,
    stream,
    rows,
    hid,
    part,
    mid,
    fin,
    vt,
    tt,
    arow,
    num,
    den,
    lsem,
    wss,
    wsr,
    oss,
    osr,
    sss,
    ssr,
    ass,
    asr,
    gss,
    gsr,
    rss,
    rsr,
):
    z, y, c, x = (lax.axis_index(n) for n in SP_TP)
    me = (z * 4 + y) * 2 + c

    def step(a, by):
        return lax.rem(a + by + 8, 4)

    def sp_device(ahead):
        i = lax.rem(me + ahead + 32, 32)
        return {"sp_0": i // 8, "sp_1": lax.rem(i // 2, 4), "sp_2": lax.rem(i, 2)}

    sibling = {"sp_2": 1 - c}
    peers = [sibling]
    for name, at in (("sp_0", z), ("sp_1", y), ("tp", x)):
        peers += [{name: step(at, 1)}, {name: step(at, -1)}]
    peers += [{"tp": step(x, 2)}]
    for d in range(1, LOOK + 1):
        peers += [sp_device(d), sp_device(-d)]

    local = []
    for n, (src, dst) in enumerate(
        (
            (k_hbm, k),
            (v_hbm, v),
            (wg_hbm, wg),
            (wu_hbm, wu),
            (wd_hbm, wd),
            (q_hbm, q),
            (ow_hbm, ow.at[x]),
            (og_hbm, og),
            (res_hbm, res),
        )
    ):
        copy = pltpu.make_async_copy(src, dst, lsem.at[n])
        copy.start()
        local.append(copy)
    in_k, in_v, in_wg, in_wu, in_wd, in_q, in_ow, in_og, in_res = local

    barrier = pltpu.get_barrier_semaphore()
    for peer in peers:
        pl.semaphore_signal(barrier, inc=1, device_id=peer, device_id_type=MESH)

    sent = []

    def remote(src, dst, send_sem, recv_sem, device):
        return pltpu.make_async_remote_copy(
            src_ref=src,
            dst_ref=dst,
            send_sem=send_sem,
            recv_sem=recv_sem,
            device_id=device,
            device_id_type=MESH,
        )

    def send(*args):
        copy = remote(*args)
        copy.start()
        sent.append(copy)

    def arrive(ref, send_sem, recv_sem):
        remote(ref, ref, send_sem, recv_sem, sibling).wait_recv()

    lane = lax.broadcasted_iota(jnp.int32, (8, 128), 1)
    row = lax.broadcasted_iota(jnp.int32, (8, 128), 0)
    docs = gates[32:40, :]
    last_lane = jnp.broadcast_to(docs[:, 127:128], (8, 128))
    heads = []
    vt[...] = jnp.zeros_like(vt)
    for h in range(2):
        cum = gates[16 + 8 * h : 24 + 8 * h, :]
        for s in (1, 2, 4, 8, 16, 32, 64):
            cum = cum + jnp.where(lane >= s, pltpu.roll(cum, s, 1), 0.0)
        upto = jnp.broadcast_to(cum[:, 127:128], (8, 128))
        for s in (1, 2, 4):
            upto = upto + jnp.where(row >= s, pltpu.roll(upto, s, 0), 0.0)
        cum = cum + jnp.where(row >= 1, pltpu.roll(upto, 1, 0), 0.0)
        a = gates[8 * h : 8 * h + 8, :] - cum
        m = a
        for s in (1, 2, 4, 8, 16, 32, 64):
            ok = (lane >= s) & (pltpu.roll(docs, s, 1) == docs)
            m = jnp.where(ok, jnp.maximum(m, pltpu.roll(m, s, 1)), m)
        e = jnp.broadcast_to(m[:, 127:128], (8, 128))
        for s in (1, 2, 4):
            ok = (row >= s) & (pltpu.roll(last_lane, s, 0) == last_lane)
            e = jnp.where(ok, jnp.maximum(e, pltpu.roll(e, s, 0)), e)
        ok = (row >= 1) & (pltpu.roll(last_lane, 1, 0) == docs)
        m = jnp.where(ok, jnp.maximum(m, pltpu.roll(e, 1, 0)), m)
        top = e[7:8, :]
        last = last_lane[7:8, :]
        weight = jnp.where(docs == last, jnp.exp(a - top), 0.0)
        arow[8 * h : 8 * h + 8, :] = a
        vt[8 * h : 8 * h + 8, :] = m
        vt[16 + 8 * h : 24 + 8 * h, :] = weight
        heads.append((top, upto[7:8, :], last))
    vt[32:40, :] = docs
    tt[...] = vt[...].T

    in_k.wait()
    in_v.wait()
    normers = []
    for h in range(2):
        cols = slice(h * HD, h * HD + HD)
        kw = jnp.concatenate(
            [
                k[128 * n : 128 * n + 128, cols].astype(F32)
                * tt[:, 16 + 8 * h + n : 17 + 8 * h + n]
                for n in range(8)
            ],
            axis=0,
        )
        hi, lo = split(kw)
        st_out[HD * h : HD * h + HD, :] = dot_tn(hi, v[:, cols]) + dot_tn(lo, v[:, cols])
        normers.append(jnp.sum(kw, axis=0, keepdims=True))
    st_out[256:264, :] = jnp.concatenate(
        normers
        + [heads[0][0], heads[1][0], heads[0][1], heads[1][1], heads[0][2], heads[0][2]],
        axis=0,
    )

    pl.semaphore_wait(barrier, len(peers))
    for d in range(1, LOOK + 1):
        send(st_out, st_in.at[d - 1], sss.at[d - 1], ssr.at[d - 1], sp_device(d))

    in_wg.wait()
    in_wu.wait()
    in_wd.wait()
    unit = (
        lax.broadcasted_iota(jnp.int32, (64, 64), 0) == lax.broadcasted_iota(jnp.int32, (64, 64), 1)
    ).astype(BF)
    for j in range(NJ):
        cols = slice(128 * j, 128 * j + 128)
        w[2 * j, z, y, c] = wg[:, cols]
        w[2 * j + 1, z, y, c] = wu[:, cols]
        w[2 * NJ + j, z, y, c] = dot_nt(unit, wd[cols, :]).astype(BF)

    def w_axes(p):
        return (("sp_0", z), ("sp_1", y)) if p == 0 else (("sp_1", y), ("sp_0", z))

    def w_at(p, first, count, uu, vv):
        zz, yy = (uu, vv) if p == 0 else (vv, uu)
        return w.at[pl.ds(first, count), zz, yy, c]

    def w_send(p, n, first, count, uu, vv, device):
        ref = w_at(p, first, count, uu, vv)
        send(ref, ref, wss.at[p, n], wsr.at[p, n], device)

    def w_arrive(p, n, first, count, uu, vv):
        arrive(w_at(p, first, count, uu, vv), wss.at[p, n], wsr.at[p, n])

    LINE = (0, -1, 1, 2)

    def w_spread(p, n):
        (_, uu), (vn, vv) = w_axes(p)
        first, count, _ = PARTS[p]
        for s, by in ((0, 1), (1, -1)):
            w_send(p, 4 + 4 * n + s, first, count, step(uu, LINE[n]), vv, {vn: step(vv, by)})

    def w_pass_on(p, n):
        (_, uu), (vn, vv) = w_axes(p)
        first, count, half = PARTS[p]
        k_at = step(uu, LINE[n])
        w_arrive(p, 4 + 4 * n, first, count, k_at, step(vv, -1))
        w_send(p, 6 + 4 * n, first, half, k_at, step(vv, -1), {vn: step(vv, 1)})
        w_arrive(p, 5 + 4 * n, first, count, k_at, step(vv, 1))
        w_send(p, 7 + 4 * n, first + half, count - half, k_at, step(vv, 1), {vn: step(vv, -1)})

    def w_line(p, n, get):
        (_, uu), _ = w_axes(p)
        first, count, _ = PARTS[p]
        k_at = step(uu, LINE[n])
        core = 1 - c if get else c
        span = pl.ds(first, count)
        ref = w.at[span, k_at, :, core] if p == 0 else w.at[span, :, k_at, core]
        if get:
            arrive(ref, wss.at[p, 20 + n], wsr.at[p, 20 + n])
        else:
            send(ref, ref, wss.at[p, 20 + n], wsr.at[p, 20 + n], sibling)

    def w_finish(p, n):
        (_, uu), (_, vv) = w_axes(p)
        first, count, half = PARTS[p]
        k_at = step(uu, LINE[n])
        w_arrive(p, 6 + 4 * n, first, half, k_at, step(vv, 2))
        w_arrive(p, 7 + 4 * n, first + half, count - half, k_at, step(vv, 2))
        w_line(p, n, False)

    def w_0(p):
        (un, uu), (_, vv) = w_axes(p)
        first, count, _ = PARTS[p]
        for s, by in ((0, 1), (1, -1)):
            w_send(p, s, first, count, uu, vv, {un: step(uu, by)})
        w_spread(p, 0)

    def w_1(p):
        (un, uu), (_, vv) = w_axes(p)
        first, count, half = PARTS[p]
        w_arrive(p, 0, first, count, step(uu, -1), vv)
        w_send(p, 2, first, half, step(uu, -1), vv, {un: step(uu, 1)})
        w_spread(p, 1)
        w_arrive(p, 1, first, count, step(uu, 1), vv)
        w_send(p, 3, first + half, count - half, step(uu, 1), vv, {un: step(uu, -1)})
        w_spread(p, 2)

    def w_2(p):
        (_, uu), (_, vv) = w_axes(p)
        first, count, half = PARTS[p]
        w_arrive(p, 2, first, half, step(uu, 2), vv)
        w_arrive(p, 3, first + half, count - half, step(uu, 2), vv)
        w_spread(p, 3)

    right, left, across = {"tp": step(x, 1)}, {"tp": step(x, -1)}, {"tp": step(x, 2)}
    x_r, x_l, x_a = step(x, 1), step(x, -1), step(x, 2)

    def o_at(slot, part_first, count):
        return ow.at[slot, pl.ds(c * 128 + part_first, count)]

    def o_send(n, slot, first, count, device):
        send(o_at(slot, first, count), o_at(slot, first, count), oss.at[n], osr.at[n], device)

    def o_arrive(n, slot, first, count):
        arrive(o_at(slot, first, count), oss.at[n], osr.at[n])

    in_ow.wait()
    o_send(0, x, 0, 128, right)
    o_send(1, x, 0, 128, left)
    w_0(0)
    w_0(1)

    in_q.wait()
    scale = HD**-0.5
    for h in range(2):
        cols = slice(h * HD, h * HD + HD)
        for i in range(4):
            at = slice(256 * i, 256 * i + 256)
            m_col, d_col = (
                jnp.concatenate([tt[:, n + 2 * i : n + 2 * i + 1], tt[:, n + 2 * i + 1 : n + 2 * i + 2]], axis=0)
                for n in (8 * h, 32)
            )
            total = jnp.zeros((256, 1), F32)
            acc = jnp.zeros((256, HD), F32)
            for j in range(i + 1):
                keys = slice(256 * j, 256 * j + 256)
                a_row = jnp.concatenate(
                    [arow[8 * h + 2 * j + s : 8 * h + 2 * j + s + 1, :] for s in range(2)], axis=1
                )
                d_row = jnp.concatenate(
                    [gates[32 + 2 * j + s : 33 + 2 * j + s, :] for s in range(2)], axis=1
                )
                ok = d_col == d_row
                if i == j:
                    ok = ok & (
                        lax.broadcasted_iota(jnp.int32, (256, 256), 0)
                        >= lax.broadcasted_iota(jnp.int32, (256, 256), 1)
                    )
                p = jnp.where(ok, dot_nt(q[at, cols], k[keys, cols]) * jnp.exp(a_row - m_col), 0.0)
                total = total + jnp.sum(p, axis=1, keepdims=True)
                hi, lo = split(p)
                acc = acc + (dot(hi, v[keys, cols]) + dot(lo, v[keys, cols]))
            num[at, cols] = acc
            den[at, cols] = jnp.broadcast_to(total, (256, HD))

    for d in range(1, LOOK + 1):
        arrive(st_in.at[d - 1], sss.at[d - 1], ssr.at[d - 1])
    in_og.wait()
    one_back = st_in[0, 262:263, :]
    carry_doc = jnp.where(me > 0, one_back, -1.0)[:, :1]
    for h in range(2):
        cols = slice(h * HD, h * HD + HD)
        passed = jnp.zeros((1, 128), F32)
        levels = []
        stab = jnp.full((1, 128), NEG, F32)
        for d in range(1, LOOK + 1):
            passed = passed + st_in[d - 1, 260 + h : 261 + h, :]
            ok = (st_in[d - 1, 262:263, :] == one_back) & (me >= d)
            level = jnp.where(ok, st_in[d - 1, 258 + h : 259 + h, :] + passed, NEG)
            levels.append(level)
            stab = jnp.maximum(stab, level)
        memory = jnp.zeros((HD, HD), F32)
        normer = jnp.zeros((1, HD), F32)
        for d in range(1, LOOK + 1):
            share = jnp.where(levels[d - 1] > 0.5 * NEG, jnp.exp(levels[d - 1] - stab), 0.0)
            memory = memory + share * st_in[d - 1, HD * h : HD * h + HD, :]
            normer = normer + share * st_in[d - 1, 256 + h : 257 + h, :]
        mem_hi, mem_lo = split(memory)
        before = stab[:, :1]
        for i in range(4):
            at = slice(256 * i, 256 * i + 256)
            m_col, d_col = (
                jnp.concatenate([tt[:, n + 2 * i : n + 2 * i + 1], tt[:, n + 2 * i + 1 : n + 2 * i + 2]], axis=0)
                for n in (8 * h, 32)
            )
            goes_on = d_col == carry_doc
            both = jnp.where(goes_on, jnp.maximum(m_col, before), m_col)
            scale_in = jnp.exp(m_col - both)
            scale_by = jnp.where(goes_on, jnp.exp(before - both), 0.0)
            queries = q[at, cols]
            from_norm = jnp.sum(queries.astype(F32) * normer, axis=1, keepdims=True)
            above = scale_in * num[at, cols] + scale_by * (dot(queries, mem_hi) + dot(queries, mem_lo))
            below = scale_in * den[at, cols] + scale_by * from_norm
            cell = above * scale / jnp.maximum(jnp.abs(below) * scale, 1.0)
            gate = 1.0 / (1.0 + jnp.exp(-og[at, cols].astype(F32)))
            gate_out[i, :, cols] = (cell * gate).astype(BF)

    for n, (device, slot) in enumerate(((right, x_r), (left, x_l), (across, x_a))):
        send(gate_out.at[slot], gate_in.at[x], ass.at[n], asr.at[n], device)
    gate_in[x] = gate_out[x]

    w_1(0)
    w_1(1)
    o_arrive(0, x_l, 0, 128)
    o_send(2, x_l, 0, 64, right)
    o_arrive(1, x_r, 0, 128)
    o_send(3, x_r, 64, 64, left)
    for n, slot in ((4, x_l), (5, x_r)):
        o_send(n, slot, 0, 128, sibling)
    w_2(0)
    w_2(1)
    w_pass_on(0, 0)
    w_pass_on(1, 0)
    o_arrive(2, x_a, 0, 64)
    o_arrive(3, x_a, 64, 64)
    o_send(6, x_a, 0, 128, sibling)
    for n, slot in enumerate((x_l, x_r, x_a)):
        arrive(gate_in.at[slot], ass.at[n], asr.at[n])
        arrive(ow.at[slot, pl.ds((1 - c) * 128, 128)], oss.at[4 + n], osr.at[4 + n])

    in_res.wait()

    def project(n, squares):
        cols = pl.ds(pl.multiple_of(n * 256, 256), 256)
        acc = res[:, cols].astype(F32)
        acc = acc + (
            (dot(gate_in[0], ow[0, :, cols]) + dot(gate_in[1], ow[1, :, cols]))
            + (dot(gate_in[2], ow[2, :, cols]) + dot(gate_in[3], ow[3, :, cols]))
        )
        stream[:, cols] = acc
        return squares + (acc[:, :128] * acc[:, :128] + acc[:, 128:] * acc[:, 128:])

    squares = lax.fori_loop(0, D // 256, project, jnp.zeros((R, 128), F32))
    inverse = lax.rsqrt(jnp.sum(squares, axis=1, keepdims=True) / D + NORM_EPS)

    def normalize(n, carry):
        cols = pl.ds(pl.multiple_of(n * 256, 256), 256)
        rows[x, :, cols] = (stream[:, cols] * inverse * gain[:, cols].astype(F32)).astype(BF)
        return carry

    lax.fori_loop(0, D // 256, normalize, 0)

    def r_at(slot, half):
        return rows.at[slot, pl.ds(128 * half, 128)]

    def r_send(n, slot, half, device):
        send(r_at(slot, half), r_at(slot, half), gss.at[n], gsr.at[n], device)

    def r_arrive(n, slot, half):
        arrive(r_at(slot, half), gss.at[n], gsr.at[n])

    r_send(0, x, 0, right)
    r_send(1, x, 1, left)
    r_send(2, x, 1, right)
    r_send(3, x, 0, left)

    for n in (1, 2):
        w_pass_on(0, n)
        w_pass_on(1, n)
    r_arrive(0, x_l, 0)
    r_send(4, x_l, 0, right)
    r_arrive(1, x_r, 1)
    r_send(5, x_r, 1, left)
    w_pass_on(0, 3)
    w_pass_on(1, 3)
    for n in range(4):
        w_finish(0, n)
        w_finish(1, n)
    for n in range(4):
        w_line(0, n, True)
        w_line(1, n, True)

    def widen(slot):
        def one(j, carry):
            both = jnp.concatenate(
                [w[2 * j].reshape(D, 128), w[2 * j + 1].reshape(D, 128)], axis=1
            )
            acts = dot(rows[slot], both)
            gate_act, up_act = acts[:, :128], acts[:, 128:]
            cols = pl.ds(pl.multiple_of(j * 128, 128), 128)
            hid[slot, :, cols] = (gate_act * (1.0 / (1.0 + jnp.exp(-gate_act))) * up_act).astype(BF)
            return carry

        lax.fori_loop(0, NJ, one, 0)

    def narrow(slot, store):
        def one(n, carry):
            down = jnp.concatenate(
                [
                    w[2 * NJ + j, n // 2, pl.ds(2 * lax.rem(n, 2), 2)].reshape(256, 128)
                    for j in range(NJ)
                ],
                axis=1,
            )
            store(pl.ds(pl.multiple_of(n * 256, 256), 256), dot_nt(hid[slot], down))
            return carry

        lax.fori_loop(0, D // 256, one, 0)

    def keep(n):
        def store(cols, value):
            part[n, :, cols] = value.astype(BF)

        return store

    widen(x)
    r_arrive(2, x_l, 1)
    widen(x_l)
    r_arrive(3, x_r, 0)
    widen(x_r)
    r_arrive(4, x_a, 0)
    r_arrive(5, x_a, 1)
    widen(x_a)

    up_half, low_half = pl.ds(0, 128), pl.ds(128, 128)
    narrow(x_a, keep(0))
    send(part.at[0, up_half], mid.at[0], rss.at[0], rsr.at[0], right)
    send(part.at[0, low_half], mid.at[1], rss.at[1], rsr.at[1], left)
    narrow(x_r, keep(1))
    send(part.at[1, low_half], fin.at[0, low_half], rss.at[2], rsr.at[2], right)
    narrow(x_l, keep(2))
    send(part.at[2, up_half], fin.at[1, up_half], rss.at[3], rsr.at[3], left)
    arrive(mid.at[0], rss.at[0], rsr.at[0])
    part[1, up_half] = (part[1, up_half].astype(F32) + mid[0].astype(F32)).astype(BF)
    send(part.at[1, up_half], fin.at[0, up_half], rss.at[4], rsr.at[4], right)
    arrive(mid.at[1], rss.at[1], rsr.at[1])
    part[2, low_half] = (part[2, low_half].astype(F32) + mid[1].astype(F32)).astype(BF)
    send(part.at[2, low_half], fin.at[1, low_half], rss.at[5], rsr.at[5], left)

    def own(cols, value):
        stream[:, cols] = stream[:, cols] + 0.5 * value

    narrow(x, own)
    arrive(fin.at[0, low_half], rss.at[2], rsr.at[2])
    arrive(fin.at[1, up_half], rss.at[3], rsr.at[3])
    arrive(fin.at[0, up_half], rss.at[4], rsr.at[4])
    arrive(fin.at[1, low_half], rss.at[5], rsr.at[5])

    def finish(n, carry):
        cols = pl.ds(pl.multiple_of(n * 256, 256), 256)
        others = fin[0, :, cols].astype(F32) + fin[1, :, cols].astype(F32)
        out[:, cols] = (stream[:, cols] + 0.5 * others).astype(BF)
        return carry

    lax.fori_loop(0, D // 256, finish, 0)
    for copy in sent:
        copy.wait_send()


def body(
    query_rows,
    key_rows,
    value_rows,
    input_gate,
    forget_gate,
    output_gate,
    documents,
    residual,
    out_weight,
    norm_gain,
    gate_weight,
    up_weight,
    down_weight,
):
    gates = jnp.concatenate(
        [
            input_gate.reshape(16, 128),
            jax.nn.log_sigmoid(forget_gate).reshape(16, 128),
            documents.astype(F32).reshape(8, 128),
        ],
        axis=0,
    )
    vmem = pl.BlockSpec(memory_space=pltpu.VMEM)
    hbm = pl.BlockSpec(memory_space=pl.ANY)
    dma = pltpu.SemaphoreType.DMA
    return pl.pallas_call(
        kernel,
        out_shape=jax.ShapeDtypeStruct((R, D), BF),
        in_specs=[vmem] * 2 + [hbm] * 9,
        out_specs=vmem,
        scratch_shapes=[
            pltpu.VMEM((T, 256), BF),
            pltpu.VMEM((T, 256), BF),
            pltpu.VMEM((T, 256), BF),
            pltpu.VMEM((T, 256), BF),
            pltpu.VMEM((R, D), BF),
            pltpu.VMEM((64, FD), BF),
            pltpu.VMEM((64, FD), BF),
            pltpu.VMEM((FD, 64), BF),
            pltpu.VMEM((TILES, 4, 4, 2, 64, 128), BF),
            pltpu.VMEM((4, 256, D), BF),
            pltpu.VMEM((264, 128), F32),
            pltpu.VMEM((LOOK, 264, 128), F32),
            pltpu.VMEM((4, R, 256), BF),
            pltpu.VMEM((4, R, 256), BF),
            pltpu.VMEM((R, D), F32),
            pltpu.VMEM((4, R, D), BF),
            pltpu.VMEM((4, R, FD), BF),
            pltpu.VMEM((3, R, D), BF),
            pltpu.VMEM((2, 128, D), BF),
            pltpu.VMEM((2, R, D), BF),
            pltpu.VMEM((128, 128), F32),
            pltpu.VMEM((128, 128), F32),
            pltpu.VMEM((16, 128), F32),
            pltpu.VMEM((T, 256), F32),
            pltpu.VMEM((T, 256), F32),
            dma((9,)),
            dma((2, 24)),
            dma((2, 24)),
            dma((7,)),
            dma((7,)),
            dma((LOOK,)),
            dma((LOOK,)),
            dma((3,)),
            dma((3,)),
            dma((6,)),
            dma((6,)),
            dma((6,)),
            dma((6,)),
        ],
        compiler_params=pltpu.CompilerParams(
            collective_id=0, has_side_effects=True, vmem_limit_bytes=62 * 1024 * 1024
        ),
    )(
        gates,
        norm_gain.reshape(1, D),
        query_rows,
        key_rows,
        value_rows,
        output_gate,
        residual,
        out_weight,
        gate_weight,
        up_weight,
        down_weight,
    )


def solution(mesh):
    torus = Mesh(mesh.devices.reshape(4, 4, 2, mesh.shape["tp"]), SP_TP)
    in_specs = (
        P(SP, "tp"),
        P(SP, "tp"),
        P(SP, "tp"),
        P("tp", SP),
        P("tp", SP),
        P(SP, "tp"),
        P(SP),
        P(SP_TP, None),
        P("tp", None),
        P(),
        P(SP, "tp"),
        P(SP, "tp"),
        P("tp", SP),
    )
    out_specs = P(SP_TP, None)
    return jax.shard_map(body, mesh=torus, in_specs=in_specs, out_specs=out_specs, check_vma=False)
```

time: 451 us -> 153 us (0.34)
  waiting for transfers between devices: 183 us -> 0 us
  Pallas kernels: 0 us -> 145 us
  local copies, waits for them, and re-layouts: 78.3 us -> 5.52 us
  matrix products: 58.1 us -> 0 us
  blocking collectives: 42.2 us -> 0 us
  other arithmetic: 39.2 us -> 1.33 us
  between operations: 32.8 us -> 0.03 us
  loops' own time: 10.8 us -> 0 us
    pallas_call x0 -> x1, Pallas kernels: none -> 145 us  [body(): pl.pallas_call(kernel, out_shape=jax.ShapeDtypeStruct((R, D), BF), in_spe...]
    all_gather x3 -> x0, waiting for transfers between devices: 130 us -> none  [the longest x1 77.2 us: gather_turned(): lax.all_gather(both, axis, axis=0, tiled=True)]
    dot_general x53 -> x0, matrix products: 58.1 us -> none  [the longest x1 22.7 us: body(): jnp.dot(hidden, whole_down, preferred_element_type=jnp.float32)]
    reduce_scatter x1 -> x0, waiting for transfers between devices: 45.9 us -> none  [body(): lax.psum_scatter(partial_sum.astype(jnp.bfloat16), 'tp', scatter_dimensio...]
    dynamic_update_slice x16 -> x0, local copies, waits for them, and re-layouts: 38.7 us -> none  [run_blocks(): final, outputs = lax.scan(block_step, start_state, inputs)]
    all_gather x3 -> x0, blocking collectives: 26.6 us -> none  [all_in_one(): both, at, found = (lax.all_gather(jnp.concatenate(lines), axis), 0, {})]
    unnamed x3 -> x0, blocking collectives: 15.6 us -> none
    dynamic_slice x16 -> x0, local copies, waits for them, and re-layouts: 14.8 us -> none  [run_blocks(): final, outputs = lax.scan(block_step, start_state, inputs)]
  transfers between devices with their start and end apart: 5 -> 0, of which waited for: 4 -> 0; matrix products, arithmetic and copies ran while one was open for 30% -> 0% of each run, Pallas kernels for 0% -> 0%
where the time goes in v1:
time: 153 us; the launch traced here: 152 us
  Pallas kernels  145 us (95%)
  local copies, waits for them, and re-layouts  5.52 us (4%)
    pallas_call x1, Pallas kernels, body(): pl.pallas_call(kernel, out_shape=jax.ShapeDtypeStruct((R, D), BF), in_spe...  145 us
    unnamed x8, local copies, waits for them, and re-layouts  4.9 us

profile of v1, /device:TPU:1, one launch (start us, length us, event | category | flops | bytes accessed | tf_op | source)
XLA Modules:
  0.0 152.3 jit_solution(11875347747954749430)
XLA Ops:
  0.0 0.0 copy-start
  0.0 0.7 convert_bitcast_fusion
  0.7 0.0 copy-done
  0.7 0.0 copy-start.1
  0.7 0.7 copy-done.1
  1.5 0.0 copy-start.2
  1.5 0.6 pad_maximum_fusion.gates
  2.1 0.1 copy-done.2
  2.1 0.6 reshape.15.gain
  2.7 1.8 %copy.14.wd_hbm = bf16[1408,64]{1,0:T(8,128)(2,1)} copy(bf16[1408,64]{0,1:T(8,128)(2,1)} %param.25) | data formatting | bytes 360448 | tf_op args[12]
  4.6 145.4 %shard_map.127 = bf16[256,2048]{1,0:T(8,128)(2,1)} custom-call(f32[40,128]{1,0:T(8,128)} %pad_maximum_fusion.gates, bf16[1,2048]{1,0:T(2,128)(2,1)} %reshape.15.gain, bf16[1024,256]{1,0:T(8,128)(2,1)} %q_hbm.1, bf16[1024,256]{1,0:T(8,128)(2,1)} %k_hbm.1, bf16[1024,256]{1,0:T(8,128)(2,1)} %v_hbm.1, bf16[1024,256]{1,0:T(8,128)(2,1)} %og_hbm.1, ...), custom_call_target="tpu_custom_call" | custom-call | tf_op jit(solution)/shard_map/pallas_call | solution.py:577
  149.9 2.3 %copy.16 = bf16[256,2048]{1,0:T(8,128)(2,1)} copy(bf16[256,2048]{1,0:T(8,128)(2,1)} %shard_map.127) | data formatting | bytes 2097152
  (3 shorter events, 0.0 us)
Async XLA Ops:
  0.0 0.7 copy-start
  0.7 0.7 copy-start.1
  1.5 0.7 copy-start.2

commit v2 on v1

--- a/solution.py
+++ b/solution.py
@@ -20,7 +20,7 @@
 D = 2048
 FD = 1408
 NJ = FD // 128
-LOOK = 6
+LOOK = 3
 TILES = 3 * NJ
 PARTS = ((0, 16, 8), (16, 17, 9))
 
@@ -43,7 +43,9 @@
 
 
 def kernel(
-    gates,
+    in_gate,
+    forget,
+    doc_ref,
     gain,
     q_hbm,
     k_hbm,
@@ -66,7 +68,11 @@
     w,
     ow,
     st_out,
-    st_in,
+    st_twin,
+    mem_out,
+    meta_out,
+    mem_in,
+    meta_in,
     gate_out,
     gate_in,
     stream,
@@ -78,8 +84,11 @@
     vt,
     tt,
     arow,
-    num,
-    den,
+    drow,
+    gsc,
+    vones,
+    numden,
+    opened,
     lsem,
     wss,
     wsr,
@@ -95,14 +104,15 @@
     rsr,
 ):
     z, y, c, x = (lax.axis_index(n) for n in SP_TP)
-    me = (z * 4 + y) * 2 + c
 
     def step(a, by):
         return lax.rem(a + by + 8, 4)
 
-    def sp_device(ahead):
-        i = lax.rem(me + ahead + 32, 32)
-        return {"sp_0": i // 8, "sp_1": lax.rem(i // 2, 4), "sp_2": lax.rem(i, 2)}
+    chip = z * 4 + y
+
+    def chip_ahead(by):
+        i = lax.rem(chip + by + 16, 16)
+        return {"sp_0": i // 4, "sp_1": lax.rem(i, 4)}
 
     sibling = {"sp_2": 1 - c}
     peers = [sibling]
@@ -110,7 +120,7 @@
         peers += [{name: step(at, 1)}, {name: step(at, -1)}]
     peers += [{"tp": step(x, 2)}]
     for d in range(1, LOOK + 1):
-        peers += [sp_device(d), sp_device(-d)]
+        peers += [chip_ahead(d), chip_ahead(-d)]
 
     local = []
     for n, (src, dst) in enumerate(
@@ -157,19 +167,26 @@
 
     lane = lax.broadcasted_iota(jnp.int32, (8, 128), 1)
     row = lax.broadcasted_iota(jnp.int32, (8, 128), 0)
-    docs = gates[32:40, :]
+    docs = doc_ref[...].astype(F32)
+    drow[...] = docs
+    gsc[...] = gain[...].astype(F32)
     last_lane = jnp.broadcast_to(docs[:, 127:128], (8, 128))
     heads = []
     vt[...] = jnp.zeros_like(vt)
+
+    def eight_rows(ref, h):
+        return jnp.concatenate([ref[h : h + 1, 128 * n : 128 * n + 128] for n in range(8)], axis=0)
+
     for h in range(2):
-        cum = gates[16 + 8 * h : 24 + 8 * h, :]
+        cum = eight_rows(forget, h)
+        cum = jnp.minimum(cum, 0.0) - jnp.log1p(jnp.exp(-jnp.abs(cum)))
         for s in (1, 2, 4, 8, 16, 32, 64):
             cum = cum + jnp.where(lane >= s, pltpu.roll(cum, s, 1), 0.0)
         upto = jnp.broadcast_to(cum[:, 127:128], (8, 128))
         for s in (1, 2, 4):
             upto = upto + jnp.where(row >= s, pltpu.roll(upto, s, 0), 0.0)
         cum = cum + jnp.where(row >= 1, pltpu.roll(upto, 1, 0), 0.0)
-        a = gates[8 * h : 8 * h + 8, :] - cum
+        a = eight_rows(in_gate, h) - cum
         m = a
         for s in (1, 2, 4, 8, 16, 32, 64):
             ok = (lane >= s) & (pltpu.roll(docs, s, 1) == docs)
@@ -186,7 +203,8 @@
         arow[8 * h : 8 * h + 8, :] = a
         vt[8 * h : 8 * h + 8, :] = m
         vt[16 + 8 * h : 24 + 8 * h, :] = weight
-        heads.append((top, upto[7:8, :], last))
+        total = upto[7:8, :]
+        heads.append((top + total, total, m))
     vt[32:40, :] = docs
     tt[...] = vt[...].T
 
@@ -208,25 +226,47 @@
         normers.append(jnp.sum(kw, axis=0, keepdims=True))
     st_out[256:264, :] = jnp.concatenate(
         normers
-        + [heads[0][0], heads[1][0], heads[0][1], heads[1][1], heads[0][2], heads[0][2]],
+        + [heads[0][0], heads[1][0], heads[0][1], heads[1][1], last, last],
         axis=0,
     )
 
     pl.semaphore_wait(barrier, len(peers))
-    for d in range(1, LOOK + 1):
-        send(st_out, st_in.at[d - 1], sss.at[d - 1], ssr.at[d - 1], sp_device(d))
+    send(st_out, st_twin, sss.at[0], ssr.at[0], sibling)
 
     in_wg.wait()
     in_wu.wait()
     in_wd.wait()
-    unit = (
-        lax.broadcasted_iota(jnp.int32, (64, 64), 0) == lax.broadcasted_iota(jnp.int32, (64, 64), 1)
-    ).astype(BF)
     for j in range(NJ):
         cols = slice(128 * j, 128 * j + 128)
         w[2 * j, z, y, c] = wg[:, cols]
         w[2 * j + 1, z, y, c] = wu[:, cols]
-        w[2 * NJ + j, z, y, c] = dot_nt(unit, wd[cols, :]).astype(BF)
+        w[2 * NJ + j, z, y, c] = wd[:, cols]
+
+    arrive(st_twin, sss.at[0], ssr.at[0])
+    first_core = c == 0
+    mine, twin = st_out[256:264, :], st_twin[256:264, :]
+    early = jnp.where(first_core, mine, twin)
+    late = jnp.where(first_core, twin, mine)
+    goes = early[6:7, :] == late[6:7, :]
+    meta = [None] * 8
+    for h in range(2):
+        span = slice(HD * h, HD * h + HD)
+        one = jnp.where(goes, early[2 + h : 3 + h, :] + late[4 + h : 5 + h, :], NEG)
+        two = late[2 + h : 3 + h, :]
+        stab = jnp.maximum(one, two)
+        share_one = jnp.where(goes, jnp.exp(one - stab), 0.0)
+        share_two = jnp.exp(two - stab)
+        share_mine = jnp.where(first_core, share_one, share_two)
+        share_twin = jnp.where(first_core, share_two, share_one)
+        mem_out[span, :] = (share_mine * st_out[span, :] + share_twin * st_twin[span, :]).astype(BF)
+        meta[h] = share_mine * mine[h : h + 1, :] + share_twin * twin[h : h + 1, :]
+        meta[2 + h] = stab
+        meta[4 + h] = early[4 + h : 5 + h, :] + late[4 + h : 5 + h, :]
+    meta[6] = meta[7] = late[6:7, :]
+    meta_out[...] = jnp.concatenate(meta, axis=0)
+    for d in range(1, LOOK + 1):
+        send(meta_out, meta_in.at[d - 1], sss.at[2 * d], ssr.at[2 * d], chip_ahead(d))
+        send(mem_out, mem_in.at[d - 1], sss.at[2 * d - 1], ssr.at[2 * d - 1], chip_ahead(d))
 
     def w_axes(p):
         return (("sp_0", z), ("sp_1", y)) if p == 0 else (("sp_1", y), ("sp_0", z))
@@ -322,24 +362,24 @@
     w_0(1)
 
     in_q.wait()
-    scale = HD**-0.5
+    for h in range(2):
+        vones[h, :, :HD] = v[:, HD * h : HD * h + HD]
+        vones[h, :, HD:] = jnp.ones((T, HD), BF)
+
+    def column(n):
+        return jnp.concatenate([tt[:, n : n + 1], tt[:, n + 1 : n + 2]], axis=0)
+
     for h in range(2):
         cols = slice(h * HD, h * HD + HD)
         for i in range(4):
             at = slice(256 * i, 256 * i + 256)
-            m_col, d_col = (
-                jnp.concatenate([tt[:, n + 2 * i : n + 2 * i + 1], tt[:, n + 2 * i + 1 : n + 2 * i + 2]], axis=0)
-                for n in (8 * h, 32)
-            )
-            total = jnp.zeros((256, 1), F32)
-            acc = jnp.zeros((256, HD), F32)
+            m_col, d_col = column(8 * h + 2 * i), column(32 + 2 * i)
+            acc = jnp.zeros((256, 2 * HD), F32)
             for j in range(i + 1):
                 keys = slice(256 * j, 256 * j + 256)
-                a_row = jnp.concatenate(
-                    [arow[8 * h + 2 * j + s : 8 * h + 2 * j + s + 1, :] for s in range(2)], axis=1
-                )
-                d_row = jnp.concatenate(
-                    [gates[32 + 2 * j + s : 33 + 2 * j + s, :] for s in range(2)], axis=1
+                a_row, d_row = (
+                    jnp.concatenate([ref[n + 2 * j : n + 2 * j + 1, :], ref[n + 2 * j + 1 : n + 2 * j + 2, :]], axis=1)
+                    for ref, n in ((arow, 8 * h), (drow, 0))
                 )
                 ok = d_col == d_row
                 if i == j:
@@ -348,53 +388,57 @@
                         >= lax.broadcasted_iota(jnp.int32, (256, 256), 1)
                     )
                 p = jnp.where(ok, dot_nt(q[at, cols], k[keys, cols]) * jnp.exp(a_row - m_col), 0.0)
-                total = total + jnp.sum(p, axis=1, keepdims=True)
                 hi, lo = split(p)
-                acc = acc + (dot(hi, v[keys, cols]) + dot(lo, v[keys, cols]))
-            num[at, cols] = acc
-            den[at, cols] = jnp.broadcast_to(total, (256, HD))
+                acc = acc + (dot(hi, vones[h, keys, :]) + dot(lo, vones[h, keys, :]))
+            numden[h, at, :] = acc
+    in_og.wait()
+    for i in range(4):
+        at = slice(256 * i, 256 * i + 256)
+        opened[at, :] = 1.0 / (1.0 + jnp.exp(-og[at, :].astype(F32)))
 
     for d in range(1, LOOK + 1):
-        arrive(st_in.at[d - 1], sss.at[d - 1], ssr.at[d - 1])
-    in_og.wait()
-    one_back = st_in[0, 262:263, :]
-    carry_doc = jnp.where(me > 0, one_back, -1.0)[:, :1]
+        arrive(meta_in.at[d - 1], sss.at[2 * d], ssr.at[2 * d])
+        arrive(mem_in.at[d - 1], sss.at[2 * d - 1], ssr.at[2 * d - 1])
+    second_core = c == 1
+    one_back = meta_in[0, 6:7, :]
+    carry_doc = jnp.where(second_core, twin[6:7, :], jnp.where(chip > 0, one_back, -1.0))
+    scale = HD**-0.5
+    memories = []
+    for h in range(2):
+        passed = jnp.where(second_core, twin[4 + h : 5 + h, :], 0.0)
+        levels = [jnp.where(second_core, twin[2 + h : 3 + h, :], NEG)]
+        for d in range(1, LOOK + 1):
+            ok = (meta_in[d - 1, 6:7, :] == carry_doc) & (chip >= d)
+            levels.append(jnp.where(ok, meta_in[d - 1, 2 + h : 3 + h, :] + passed, NEG))
+            passed = passed + meta_in[d - 1, 4 + h : 5 + h, :]
+        stab = levels[0]
+        for level in levels[1:]:
+            stab = jnp.maximum(stab, level)
+        shares = [jnp.where(level > 0.5 * NEG, jnp.exp(level - stab), 0.0) for level in levels]
+        memory = shares[0] * st_twin[HD * h : HD * h + HD, :]
+        normer = shares[0] * twin[h : h + 1, :]
+        for d in range(1, LOOK + 1):
+            memory = memory + shares[d] * mem_in[d - 1, HD * h : HD * h + HD, :].astype(F32)
+            normer = normer + shares[d] * meta_in[d - 1, h : h + 1, :]
+        memories.append(memory)
+        m = heads[h][2]
+        goes_on = docs == carry_doc
+        both = jnp.where(goes_on, jnp.maximum(m, stab), m)
+        vt[8 * h : 8 * h + 8, :] = jnp.exp(m - both) * scale
+        vt[16 + 8 * h : 24 + 8 * h, :] = jnp.where(goes_on, jnp.exp(stab - both), 0.0) * scale
+        vt[32 + 8 * h : 40 + 8 * h, :] = jnp.broadcast_to(normer, (8, HD))
+    tt[...] = vt[...].T
     for h in range(2):
         cols = slice(h * HD, h * HD + HD)
-        passed = jnp.zeros((1, 128), F32)
-        levels = []
-        stab = jnp.full((1, 128), NEG, F32)
-        for d in range(1, LOOK + 1):
-            passed = passed + st_in[d - 1, 260 + h : 261 + h, :]
-            ok = (st_in[d - 1, 262:263, :] == one_back) & (me >= d)
-            level = jnp.where(ok, st_in[d - 1, 258 + h : 259 + h, :] + passed, NEG)
-            levels.append(level)
-            stab = jnp.maximum(stab, level)
-        memory = jnp.zeros((HD, HD), F32)
-        normer = jnp.zeros((1, HD), F32)
-        for d in range(1, LOOK + 1):
-            share = jnp.where(levels[d - 1] > 0.5 * NEG, jnp.exp(levels[d - 1] - stab), 0.0)
-            memory = memory + share * st_in[d - 1, HD * h : HD * h + HD, :]
-            normer = normer + share * st_in[d - 1, 256 + h : 257 + h, :]
-        mem_hi, mem_lo = split(memory)
-        before = stab[:, :1]
+        normer = jnp.broadcast_to(tt[:, 32 + 8 * h : 33 + 8 * h], (HD, HD))
+        parts = [jnp.concatenate(pair, axis=1) for pair in zip(split(memories[h]), split(normer))]
         for i in range(4):
             at = slice(256 * i, 256 * i + 256)
-            m_col, d_col = (
-                jnp.concatenate([tt[:, n + 2 * i : n + 2 * i + 1], tt[:, n + 2 * i + 1 : n + 2 * i + 2]], axis=0)
-                for n in (8 * h, 32)
-            )
-            goes_on = d_col == carry_doc
-            both = jnp.where(goes_on, jnp.maximum(m_col, before), m_col)
-            scale_in = jnp.exp(m_col - both)
-            scale_by = jnp.where(goes_on, jnp.exp(before - both), 0.0)
+            scale_in, scale_by = column(8 * h + 2 * i), column(16 + 8 * h + 2 * i)
             queries = q[at, cols]
-            from_norm = jnp.sum(queries.astype(F32) * normer, axis=1, keepdims=True)
-            above = scale_in * num[at, cols] + scale_by * (dot(queries, mem_hi) + dot(queries, mem_lo))
-            below = scale_in * den[at, cols] + scale_by * from_norm
-            cell = above * scale / jnp.maximum(jnp.abs(below) * scale, 1.0)
-            gate = 1.0 / (1.0 + jnp.exp(-og[at, cols].astype(F32)))
-            gate_out[i, :, cols] = (cell * gate).astype(BF)
+            both = scale_in * numden[h, at, :] + scale_by * (dot(queries, parts[0]) + dot(queries, parts[1]))
+            cell = both[:, :HD] / jnp.maximum(jnp.abs(both[:, HD:]), 1.0)
+            gate_out[i, :, cols] = (cell * opened[at, cols]).astype(BF)
 
     for n, (device, slot) in enumerate(((right, x_r), (left, x_l), (across, x_a))):
         send(gate_out.at[slot], gate_in.at[x], ass.at[n], asr.at[n], device)
@@ -408,8 +452,6 @@
     o_send(3, x_r, 64, 64, left)
     for n, slot in ((4, x_l), (5, x_r)):
         o_send(n, slot, 0, 128, sibling)
-    w_2(0)
-    w_2(1)
     w_pass_on(0, 0)
     w_pass_on(1, 0)
     o_arrive(2, x_a, 0, 64)
@@ -417,6 +459,7 @@
     o_send(6, x_a, 0, 128, sibling)
     for n, slot in enumerate((x_l, x_r, x_a)):
         arrive(gate_in.at[slot], ass.at[n], asr.at[n])
+    for n, slot in enumerate((x_l, x_r, x_a)):
         arrive(ow.at[slot, pl.ds((1 - c) * 128, 128)], oss.at[4 + n], osr.at[4 + n])
 
     in_res.wait()
@@ -436,7 +479,8 @@
 
     def normalize(n, carry):
         cols = pl.ds(pl.multiple_of(n * 256, 256), 256)
-        rows[x, :, cols] = (stream[:, cols] * inverse * gain[:, cols].astype(F32)).astype(BF)
+        gain_row = jnp.concatenate([gsc[pl.ds(2 * n, 1), :], gsc[pl.ds(2 * n + 1, 1), :]], axis=1)
+        rows[x, :, cols] = (stream[:, cols] * inverse * gain_row).astype(BF)
         return carry
 
     lax.fori_loop(0, D // 256, normalize, 0)
@@ -455,48 +499,54 @@
     r_send(2, x, 1, right)
     r_send(3, x, 0, left)
 
+    w_2(0)
+    w_2(1)
     for n in (1, 2):
         w_pass_on(0, n)
         w_pass_on(1, n)
+    w_finish(0, 0)
+    w_finish(1, 0)
     r_arrive(0, x_l, 0)
     r_send(4, x_l, 0, right)
     r_arrive(1, x_r, 1)
     r_send(5, x_r, 1, left)
     w_pass_on(0, 3)
     w_pass_on(1, 3)
-    for n in range(4):
+    for n in (1, 2, 3):
         w_finish(0, n)
         w_finish(1, n)
     for n in range(4):
         w_line(0, n, True)
         w_line(1, n, True)
 
-    def widen(slot):
+    up_half, low_half = pl.ds(0, 128), pl.ds(128, 128)
+
+    def widen(n, pieces):
         def one(j, carry):
             both = jnp.concatenate(
                 [w[2 * j].reshape(D, 128), w[2 * j + 1].reshape(D, 128)], axis=1
             )
-            acts = dot(rows[slot], both)
+            acts = dot(jnp.concatenate([rows[piece] for piece in pieces], axis=0), both)
             gate_act, up_act = acts[:, :128], acts[:, 128:]
             cols = pl.ds(pl.multiple_of(j * 128, 128), 128)
-            hid[slot, :, cols] = (gate_act * (1.0 / (1.0 + jnp.exp(-gate_act))) * up_act).astype(BF)
+            hid[n, :, cols] = (gate_act * (1.0 / (1.0 + jnp.exp(-gate_act))) * up_act).astype(BF)
             return carry
 
         lax.fori_loop(0, NJ, one, 0)
 
-    def narrow(slot, store):
-        def one(n, carry):
+    def narrow(n, store, first=0, last=D // 256):
+        def one(t, carry):
             down = jnp.concatenate(
                 [
-                    w[2 * NJ + j, n // 2, pl.ds(2 * lax.rem(n, 2), 2)].reshape(256, 128)
+                    w[2 * NJ + j, t // 2, pl.ds(2 * lax.rem(t, 2), 2)].reshape(256, 128)
                     for j in range(NJ)
                 ],
                 axis=1,
             )
-            store(pl.ds(pl.multiple_of(n * 256, 256), 256), dot_nt(hid[slot], down))
+            store(pl.ds(pl.multiple_of(t * 256, 256), 256), dot_nt(hid[n], down))
             return carry
 
-        lax.fori_loop(0, D // 256, one, 0)
+        lax.fori_loop(first, last, one, 0)
 
     def keep(n):
         def store(cols, value):
@@ -504,38 +554,48 @@
 
         return store
 
-    widen(x)
+    def p_send(n, src, dst, device):
+        send(src, dst, rss.at[n], rsr.at[n], device)
+
+    def p_arrive(n, ref):
+        arrive(ref, rss.at[n], rsr.at[n])
+
+    def piece(ref, slot, half, side):
+        return ref.at[slot, half, pl.ds(1024 * side, 1024)]
+
+    widen(0, ((x_l, up_half), (x_r, low_half)))
+    narrow(0, keep(0))
+    p_send(0, part.at[0, low_half], fin.at[0, low_half], right)
+    p_send(1, part.at[0, up_half], fin.at[1, up_half], left)
     r_arrive(2, x_l, 1)
-    widen(x_l)
     r_arrive(3, x_r, 0)
-    widen(x_r)
+    widen(1, ((x_r, up_half), (x_l, low_half)))
     r_arrive(4, x_a, 0)
     r_arrive(5, x_a, 1)
-    widen(x_a)
-
-    up_half, low_half = pl.ds(0, 128), pl.ds(128, 128)
-    narrow(x_a, keep(0))
-    send(part.at[0, up_half], mid.at[0], rss.at[0], rsr.at[0], right)
-    send(part.at[0, low_half], mid.at[1], rss.at[1], rsr.at[1], left)
-    narrow(x_r, keep(1))
-    send(part.at[1, low_half], fin.at[0, low_half], rss.at[2], rsr.at[2], right)
-    narrow(x_l, keep(2))
-    send(part.at[2, up_half], fin.at[1, up_half], rss.at[3], rsr.at[3], left)
-    arrive(mid.at[0], rss.at[0], rsr.at[0])
-    part[1, up_half] = (part[1, up_half].astype(F32) + mid[0].astype(F32)).astype(BF)
-    send(part.at[1, up_half], fin.at[0, up_half], rss.at[4], rsr.at[4], right)
-    arrive(mid.at[1], rss.at[1], rsr.at[1])
-    part[2, low_half] = (part[2, low_half].astype(F32) + mid[1].astype(F32)).astype(BF)
-    send(part.at[2, low_half], fin.at[1, low_half], rss.at[5], rsr.at[5], left)
-
+    widen(2, ((x_a, up_half), (x_a, low_half)))
+    for side in range(2):
+        narrow(2, keep(2), 4 * side, 4 * side + 4)
+        p_send(2 + 2 * side, piece(part, 2, up_half, side), piece(mid, 0, up_half, side), right)
+        p_send(3 + 2 * side, piece(part, 2, low_half, side), piece(mid, 1, up_half, side), left)
+    narrow(1, keep(1))
+    widen(3, ((x, up_half), (x, low_half)))
+    for side in range(2):
+        at = pl.ds(1024 * side, 1024)
+        p_arrive(2 + 2 * side, piece(mid, 0, up_half, side))
+        part[1, up_half, at] = (part[1, up_half, at].astype(F32) + mid[0, :, at].astype(F32)).astype(BF)
+        p_send(6 + 2 * side, piece(part, 1, up_half, side), piece(fin, 0, up_half, side), right)
+        p_arrive(3 + 2 * side, piece(mid, 1, up_half, side))
+        part[1, low_half, at] = (part[1, low_half, at].astype(F32) + mid[1, :, at].astype(F32)).astype(BF)
+        p_send(7 + 2 * side, piece(part, 1, low_half, side), piece(fin, 1, low_half, side), left)
     def own(cols, value):
         stream[:, cols] = stream[:, cols] + 0.5 * value
 
-    narrow(x, own)
-    arrive(fin.at[0, low_half], rss.at[2], rsr.at[2])
-    arrive(fin.at[1, up_half], rss.at[3], rsr.at[3])
-    arrive(fin.at[0, up_half], rss.at[4], rsr.at[4])
-    arrive(fin.at[1, low_half], rss.at[5], rsr.at[5])
+    narrow(3, own)
+    p_arrive(0, fin.at[0, low_half])
+    p_arrive(1, fin.at[1, up_half])
+    for side in range(2):
+        p_arrive(6 + 2 * side, piece(fin, 0, up_half, side))
+        p_arrive(7 + 2 * side, piece(fin, 1, low_half, side))
 
     def finish(n, carry):
         cols = pl.ds(pl.multiple_of(n * 256, 256), 256)
@@ -563,21 +623,13 @@
     up_weight,
     down_weight,
 ):
-    gates = jnp.concatenate(
-        [
-            input_gate.reshape(16, 128),
-            jax.nn.log_sigmoid(forget_gate).reshape(16, 128),
-            documents.astype(F32).reshape(8, 128),
-        ],
-        axis=0,
-    )
     vmem = pl.BlockSpec(memory_space=pltpu.VMEM)
     hbm = pl.BlockSpec(memory_space=pl.ANY)
     dma = pltpu.SemaphoreType.DMA
     return pl.pallas_call(
         kernel,
         out_shape=jax.ShapeDtypeStruct((R, D), BF),
-        in_specs=[vmem] * 2 + [hbm] * 9,
+        in_specs=[vmem] * 4 + [hbm] * 9,
         out_specs=vmem,
         scratch_shapes=[
             pltpu.VMEM((T, 256), BF),
@@ -587,11 +639,15 @@
             pltpu.VMEM((R, D), BF),
             pltpu.VMEM((64, FD), BF),
             pltpu.VMEM((64, FD), BF),
-            pltpu.VMEM((FD, 64), BF),
+            pltpu.VMEM((64, FD), BF),
             pltpu.VMEM((TILES, 4, 4, 2, 64, 128), BF),
             pltpu.VMEM((4, 256, D), BF),
             pltpu.VMEM((264, 128), F32),
-            pltpu.VMEM((LOOK, 264, 128), F32),
+            pltpu.VMEM((264, 128), F32),
+            pltpu.VMEM((256, 128), BF),
+            pltpu.VMEM((8, 128), F32),
+            pltpu.VMEM((LOOK, 256, 128), BF),
+            pltpu.VMEM((LOOK, 8, 128), F32),
             pltpu.VMEM((4, R, 256), BF),
             pltpu.VMEM((4, R, 256), BF),
             pltpu.VMEM((R, D), F32),
@@ -603,28 +659,33 @@
             pltpu.VMEM((128, 128), F32),
             pltpu.VMEM((128, 128), F32),
             pltpu.VMEM((16, 128), F32),
-            pltpu.VMEM((T, 256), F32),
+            pltpu.VMEM((8, 128), F32),
+            pltpu.VMEM((16, 128), F32),
+            pltpu.VMEM((2, T, 256), BF),
+            pltpu.VMEM((2, T, 256), F32),
             pltpu.VMEM((T, 256), F32),
             dma((9,)),
             dma((2, 24)),
             dma((2, 24)),
             dma((7,)),
             dma((7,)),
-            dma((LOOK,)),
-            dma((LOOK,)),
+            dma((2 * LOOK + 1,)),
+            dma((2 * LOOK + 1,)),
             dma((3,)),
             dma((3,)),
             dma((6,)),
             dma((6,)),
-            dma((6,)),
-            dma((6,)),
+            dma((10,)),
+            dma((10,)),
         ],
         compiler_params=pltpu.CompilerParams(
             collective_id=0, has_side_effects=True, vmem_limit_bytes=62 * 1024 * 1024
         ),
     )(
-        gates,
-        norm_gain.reshape(1, D),
+        input_gate,
+        forget_gate,
+        documents.reshape(8, 128),
+        norm_gain.reshape(16, 128),
         query_rows,
         key_rows,
         value_rows,
@@ -633,7 +694,7 @@
         out_weight,
         gate_weight,
         up_weight,
-        down_weight,
+        down_weight.T,
     )
 
 

time: 153 us -> 116 us (0.76)
  Pallas kernels: 145 us -> 113 us
  local copies, waits for them, and re-layouts: 5.52 us -> 2.3 us
    pallas_call x1, Pallas kernels: 145 us -> 113 us  [body(): pl.pallas_call(kernel, out_shape=jax.ShapeDtypeStruct((R, D), BF), in_spe...]
    unnamed x8 -> x1, local copies, waits for them, and re-layouts: 4.9 us -> 2.3 us
where the time goes in v2:
time: 116 us; the launch traced here: 115 us
  Pallas kernels  113 us (97%)
  local copies, waits for them, and re-layouts  2.3 us (2%)
    pallas_call x1, Pallas kernels, body(): pl.pallas_call(kernel, out_shape=jax.ShapeDtypeStruct((R, D), BF), in_spe...  113 us

profile of v2, /device:TPU:1, one launch (start us, length us, event | category | flops | bytes accessed | tf_op | source)
XLA Modules:
  0.0 115.4 jit_solution(3490917979200874348)
XLA Ops:
  0.0 113.1 %shard_map.127 = bf16[256,2048]{1,0:T(8,128)(2,1)} custom-call(f32[2,1024]{1,0:T(2,128)} %in_gate.1, f32[2,1024]{1,0:T(2,128)} %forget.1, s32[8,128]{1,0:T(8,128)} %bitcast.4, bf16[16,128]{1,0:T(8,128)(2,1)} %bitcast.5, bf16[1024,256]{1,0:T(8,128)(2,1)} %q_hbm.1, bf16[1024,256]{1,0:T(8,128)(2,1)} %k_hbm.1, bf16[1024,256]{1,0:T(8,128)(2,1)} %v_hbm.1, ...), custom_call_target="tpu_custom_call" | custom-call | tf_op jit(solution)/shard_map/pallas_call | solution.py:629
  113.1 2.3 %copy.15 = bf16[256,2048]{1,0:T(8,128)(2,1)} copy(bf16[256,2048]{1,0:T(8,128)(2,1)} %shard_map.127) | data formatting | bytes 2097152

commit v3 on v2

--- a/solution.py
+++ b/solution.py
@@ -22,7 +22,7 @@
 NJ = FD // 128
 LOOK = 3
 TILES = 3 * NJ
-PARTS = ((0, 16, 8), (16, 17, 9))
+PARTS = ((0, 9, 5), (9, 13, 6), (22, 5, 3), (27, 6, 3))
 
 
 def dot(a, b):
@@ -43,10 +43,10 @@
 
 
 def kernel(
-    in_gate,
-    forget,
-    doc_ref,
-    gain,
+    in_gate_hbm,
+    forget_hbm,
+    doc_hbm,
+    gain_hbm,
     q_hbm,
     k_hbm,
     v_hbm,
@@ -57,6 +57,10 @@
     wu_hbm,
     wd_hbm,
     out,
+    in_gate,
+    forget,
+    doc_ref,
+    gain,
     q,
     k,
     v,
@@ -75,6 +79,7 @@
     meta_in,
     gate_out,
     gate_in,
+    gate_relay,
     stream,
     rows,
     hid,
@@ -122,16 +127,24 @@
     for d in range(1, LOOK + 1):
         peers += [chip_ahead(d), chip_ahead(-d)]
 
+    barrier = pltpu.get_barrier_semaphore()
+    for peer in peers:
+        pl.semaphore_signal(barrier, inc=1, device_id=peer, device_id_type=MESH)
+
     local = []
     for n, (src, dst) in enumerate(
         (
-            (k_hbm, k),
-            (v_hbm, v),
+            (in_gate_hbm, in_gate),
+            (forget_hbm, forget),
+            (doc_hbm, doc_ref),
+            (gain_hbm, gain),
+            (ow_hbm, ow.at[x]),
             (wg_hbm, wg),
             (wu_hbm, wu),
             (wd_hbm, wd),
+            (k_hbm, k),
+            (v_hbm, v),
             (q_hbm, q),
-            (ow_hbm, ow.at[x]),
             (og_hbm, og),
             (res_hbm, res),
         )
@@ -139,11 +152,7 @@
         copy = pltpu.make_async_copy(src, dst, lsem.at[n])
         copy.start()
         local.append(copy)
-    in_k, in_v, in_wg, in_wu, in_wd, in_q, in_ow, in_og, in_res = local
-
-    barrier = pltpu.get_barrier_semaphore()
-    for peer in peers:
-        pl.semaphore_signal(barrier, inc=1, device_id=peer, device_id_type=MESH)
+    small, (in_ow, in_wg, in_wu, in_wd, in_k, in_v, in_q, in_og, in_res) = local[:4], local[4:]
 
     sent = []
 
@@ -165,6 +174,117 @@
     def arrive(ref, send_sem, recv_sem):
         remote(ref, ref, send_sem, recv_sem, sibling).wait_recv()
 
+    def w_axes(p):
+        return (("sp_0", z), ("sp_1", y)) if p % 2 == 0 else (("sp_1", y), ("sp_0", z))
+
+    def w_at(p, first, count, uu, vv):
+        zz, yy = (uu, vv) if p % 2 == 0 else (vv, uu)
+        return w.at[pl.ds(first, count), zz, yy, c]
+
+    def w_send(p, n, first, count, uu, vv, device):
+        ref = w_at(p, first, count, uu, vv)
+        send(ref, ref, wss.at[p, n], wsr.at[p, n], device)
+
+    def w_arrive(p, n, first, count, uu, vv):
+        arrive(w_at(p, first, count, uu, vv), wss.at[p, n], wsr.at[p, n])
+
+    LINE = (0, -1, 1, 2)
+
+    def w_spread(p, n):
+        (_, uu), (vn, vv) = w_axes(p)
+        first, count, _ = PARTS[p]
+        for s, by in ((0, 1), (1, -1)):
+            w_send(p, 4 + 4 * n + s, first, count, step(uu, LINE[n]), vv, {vn: step(vv, by)})
+
+    def w_pass_on(p, n):
+        (_, uu), (vn, vv) = w_axes(p)
+        first, count, half = PARTS[p]
+        k_at = step(uu, LINE[n])
+        w_arrive(p, 4 + 4 * n, first, count, k_at, step(vv, -1))
+        w_send(p, 6 + 4 * n, first, half, k_at, step(vv, -1), {vn: step(vv, 1)})
+        w_arrive(p, 5 + 4 * n, first, count, k_at, step(vv, 1))
+        w_send(p, 7 + 4 * n, first + half, count - half, k_at, step(vv, 1), {vn: step(vv, -1)})
+
+    def w_line(p, n, get):
+        (_, uu), _ = w_axes(p)
+        first, count, _ = PARTS[p]
+        k_at = step(uu, LINE[n])
+        core = 1 - c if get else c
+        span = pl.ds(first, count)
+        ref = w.at[span, k_at, :, core] if p % 2 == 0 else w.at[span, :, k_at, core]
+        if get:
+            arrive(ref, wss.at[p, 20 + n], wsr.at[p, 20 + n])
+        else:
+            send(ref, ref, wss.at[p, 20 + n], wsr.at[p, 20 + n], sibling)
+
+    def w_finish(p, n):
+        (_, uu), (_, vv) = w_axes(p)
+        first, count, half = PARTS[p]
+        k_at = step(uu, LINE[n])
+        w_arrive(p, 6 + 4 * n, first, half, k_at, step(vv, 2))
+        w_arrive(p, 7 + 4 * n, first + half, count - half, k_at, step(vv, 2))
+        w_line(p, n, False)
+
+    def w_0(name):
+        for p in (0, 1, 2, 3) if name == "sp_0" else (1, 0, 3, 2):
+            (un, uu), (_, vv) = w_axes(p)
+            first, count, _ = PARTS[p]
+            if un == name:
+                for n, by in ((0, 1), (1, -1)):
+                    w_send(p, n, first, count, uu, vv, {un: step(uu, by)})
+            else:
+                w_spread(p, 0)
+
+    def w_1(p):
+        (un, uu), (_, vv) = w_axes(p)
+        first, count, half = PARTS[p]
+        w_arrive(p, 0, first, count, step(uu, -1), vv)
+        w_send(p, 2, first, half, step(uu, -1), vv, {un: step(uu, 1)})
+        w_spread(p, 1)
+        w_arrive(p, 1, first, count, step(uu, 1), vv)
+        w_send(p, 3, first + half, count - half, step(uu, 1), vv, {un: step(uu, -1)})
+        w_spread(p, 2)
+
+    def w_2(p):
+        (_, uu), (_, vv) = w_axes(p)
+        first, count, half = PARTS[p]
+        w_arrive(p, 2, first, half, step(uu, 2), vv)
+        w_arrive(p, 3, first + half, count - half, step(uu, 2), vv)
+        w_spread(p, 3)
+
+    right, left, across = {"tp": step(x, 1)}, {"tp": step(x, -1)}, {"tp": step(x, 2)}
+    x_r, x_l, x_a = step(x, 1), step(x, -1), step(x, 2)
+
+    def o_at(slot, part_first, count):
+        return ow.at[slot, pl.ds(c * 128 + part_first, count)]
+
+    def o_send(n, slot, first, count, device):
+        send(o_at(slot, first, count), o_at(slot, first, count), oss.at[n], osr.at[n], device)
+
+
+    def o_arrive(n, slot, first, count):
+        arrive(o_at(slot, first, count), oss.at[n], osr.at[n])
+
+    pl.semaphore_wait(barrier, len(peers))
+    in_ow.wait()
+    o_send(0, x, 0, 64, right)
+    o_send(1, x, 64, 64, left)
+    o_send(2, x, 64, 64, right)
+    o_send(3, x, 0, 64, left)
+
+    in_wg.wait()
+    in_wu.wait()
+    in_wd.wait()
+    for j in range(NJ):
+        cols = slice(128 * j, 128 * j + 128)
+        w[2 * j, z, y, c] = wg[:, cols]
+        w[2 * j + 1, z, y, c] = wu[:, cols]
+        w[2 * NJ + j, z, y, c] = wd[:, cols]
+
+    w_0("sp_0")
+
+    for copy in small:
+        copy.wait()
     lane = lax.broadcasted_iota(jnp.int32, (8, 128), 1)
     row = lax.broadcasted_iota(jnp.int32, (8, 128), 0)
     docs = doc_ref[...].astype(F32)
@@ -230,17 +350,7 @@
         axis=0,
     )
 
-    pl.semaphore_wait(barrier, len(peers))
     send(st_out, st_twin, sss.at[0], ssr.at[0], sibling)
-
-    in_wg.wait()
-    in_wu.wait()
-    in_wd.wait()
-    for j in range(NJ):
-        cols = slice(128 * j, 128 * j + 128)
-        w[2 * j, z, y, c] = wg[:, cols]
-        w[2 * j + 1, z, y, c] = wu[:, cols]
-        w[2 * NJ + j, z, y, c] = wd[:, cols]
 
     arrive(st_twin, sss.at[0], ssr.at[0])
     first_core = c == 0
@@ -264,102 +374,12 @@
         meta[4 + h] = early[4 + h : 5 + h, :] + late[4 + h : 5 + h, :]
     meta[6] = meta[7] = late[6:7, :]
     meta_out[...] = jnp.concatenate(meta, axis=0)
+    head = pl.ds(HD * c, HD)
     for d in range(1, LOOK + 1):
         send(meta_out, meta_in.at[d - 1], sss.at[2 * d], ssr.at[2 * d], chip_ahead(d))
-        send(mem_out, mem_in.at[d - 1], sss.at[2 * d - 1], ssr.at[2 * d - 1], chip_ahead(d))
-
-    def w_axes(p):
-        return (("sp_0", z), ("sp_1", y)) if p == 0 else (("sp_1", y), ("sp_0", z))
-
-    def w_at(p, first, count, uu, vv):
-        zz, yy = (uu, vv) if p == 0 else (vv, uu)
-        return w.at[pl.ds(first, count), zz, yy, c]
-
-    def w_send(p, n, first, count, uu, vv, device):
-        ref = w_at(p, first, count, uu, vv)
-        send(ref, ref, wss.at[p, n], wsr.at[p, n], device)
-
-    def w_arrive(p, n, first, count, uu, vv):
-        arrive(w_at(p, first, count, uu, vv), wss.at[p, n], wsr.at[p, n])
-
-    LINE = (0, -1, 1, 2)
-
-    def w_spread(p, n):
-        (_, uu), (vn, vv) = w_axes(p)
-        first, count, _ = PARTS[p]
-        for s, by in ((0, 1), (1, -1)):
-            w_send(p, 4 + 4 * n + s, first, count, step(uu, LINE[n]), vv, {vn: step(vv, by)})
-
-    def w_pass_on(p, n):
-        (_, uu), (vn, vv) = w_axes(p)
-        first, count, half = PARTS[p]
-        k_at = step(uu, LINE[n])
-        w_arrive(p, 4 + 4 * n, first, count, k_at, step(vv, -1))
-        w_send(p, 6 + 4 * n, first, half, k_at, step(vv, -1), {vn: step(vv, 1)})
-        w_arrive(p, 5 + 4 * n, first, count, k_at, step(vv, 1))
-        w_send(p, 7 + 4 * n, first + half, count - half, k_at, step(vv, 1), {vn: step(vv, -1)})
-
-    def w_line(p, n, get):
-        (_, uu), _ = w_axes(p)
-        first, count, _ = PARTS[p]
-        k_at = step(uu, LINE[n])
-        core = 1 - c if get else c
-        span = pl.ds(first, count)
-        ref = w.at[span, k_at, :, core] if p == 0 else w.at[span, :, k_at, core]
-        if get:
-            arrive(ref, wss.at[p, 20 + n], wsr.at[p, 20 + n])
-        else:
-            send(ref, ref, wss.at[p, 20 + n], wsr.at[p, 20 + n], sibling)
-
-    def w_finish(p, n):
-        (_, uu), (_, vv) = w_axes(p)
-        first, count, half = PARTS[p]
-        k_at = step(uu, LINE[n])
-        w_arrive(p, 6 + 4 * n, first, half, k_at, step(vv, 2))
-        w_arrive(p, 7 + 4 * n, first + half, count - half, k_at, step(vv, 2))
-        w_line(p, n, False)
-
-    def w_0(p):
-        (un, uu), (_, vv) = w_axes(p)
-        first, count, _ = PARTS[p]
-        for s, by in ((0, 1), (1, -1)):
-            w_send(p, s, first, count, uu, vv, {un: step(uu, by)})
-        w_spread(p, 0)
-
-    def w_1(p):
-        (un, uu), (_, vv) = w_axes(p)
-        first, count, half = PARTS[p]
-        w_arrive(p, 0, first, count, step(uu, -1), vv)
-        w_send(p, 2, first, half, step(uu, -1), vv, {un: step(uu, 1)})
-        w_spread(p, 1)
-        w_arrive(p, 1, first, count, step(uu, 1), vv)
-        w_send(p, 3, first + half, count - half, step(uu, 1), vv, {un: step(uu, -1)})
-        w_spread(p, 2)
-
-    def w_2(p):
-        (_, uu), (_, vv) = w_axes(p)
-        first, count, half = PARTS[p]
-        w_arrive(p, 2, first, half, step(uu, 2), vv)
-        w_arrive(p, 3, first + half, count - half, step(uu, 2), vv)
-        w_spread(p, 3)
-
-    right, left, across = {"tp": step(x, 1)}, {"tp": step(x, -1)}, {"tp": step(x, 2)}
-    x_r, x_l, x_a = step(x, 1), step(x, -1), step(x, 2)
-
-    def o_at(slot, part_first, count):
-        return ow.at[slot, pl.ds(c * 128 + part_first, count)]
-
-    def o_send(n, slot, first, count, device):
-        send(o_at(slot, first, count), o_at(slot, first, count), oss.at[n], osr.at[n], device)
-
-    def o_arrive(n, slot, first, count):
-        arrive(o_at(slot, first, count), oss.at[n], osr.at[n])
-
-    in_ow.wait()
-    o_send(0, x, 0, 128, right)
-    o_send(1, x, 0, 128, left)
-    w_0(0)
-    w_0(1)
+        send(mem_out.at[head], mem_in.at[d - 1, head], sss.at[2 * d - 1], ssr.at[2 * d - 1], chip_ahead(d))
+
+    w_0("sp_1")
 
     in_q.wait()
     for h in range(2):
@@ -396,9 +416,18 @@
         at = slice(256 * i, 256 * i + 256)
         opened[at, :] = 1.0 / (1.0 + jnp.exp(-og[at, :].astype(F32)))
 
+    o_arrive(0, x_l, 0, 64)
+    o_send(4, x_l, 0, 64, right)
+    o_arrive(1, x_r, 64, 64)
+    o_send(5, x_r, 64, 64, left)
     for d in range(1, LOOK + 1):
+        arrive(mem_in.at[d - 1, head], sss.at[2 * d - 1], ssr.at[2 * d - 1])
+        n = 2 * LOOK + d
+        send(mem_in.at[d - 1, head], mem_in.at[d - 1, head], sss.at[n], ssr.at[n], sibling)
+    for d in range(1, LOOK + 1):
+        n = 2 * LOOK + d
         arrive(meta_in.at[d - 1], sss.at[2 * d], ssr.at[2 * d])
-        arrive(mem_in.at[d - 1], sss.at[2 * d - 1], ssr.at[2 * d - 1])
+        arrive(mem_in.at[d - 1, pl.ds(HD * (1 - c), HD)], sss.at[n], ssr.at[n])
     second_core = c == 1
     one_back = meta_in[0, 6:7, :]
     carry_doc = jnp.where(second_core, twin[6:7, :], jnp.where(chip > 0, one_back, -1.0))
@@ -440,64 +469,95 @@
             cell = both[:, :HD] / jnp.maximum(jnp.abs(both[:, HD:]), 1.0)
             gate_out[i, :, cols] = (cell * opened[at, cols]).astype(BF)
 
-    for n, (device, slot) in enumerate(((right, x_r), (left, x_l), (across, x_a))):
-        send(gate_out.at[slot], gate_in.at[x], ass.at[n], asr.at[n], device)
+    def half_of(ref, slot, half):
+        return ref.at[slot, pl.ds(128 * half, 128)]
+
+    onward, behind = {"tp": lax.rem(x + 1 + 2 * c, 4)}, lax.rem(x + 3 + 2 * c, 4)
+
+    def g_send(n, half, src, dst, device):
+        m = 4 * half + n
+        send(half_of(*src, half), half_of(*dst, half), ass.at[m], asr.at[m], device)
+
+    def g_arrive(n, half, ref, slot):
+        m = 4 * half + n
+        arrive(half_of(ref, slot, half), ass.at[m], asr.at[m])
+
+    for half in range(2):
+        g_send(2, half, (gate_out, x_a), (gate_relay, 0), onward)
+    for half in range(2):
+        g_send(0, half, (gate_out, x_r), (gate_in, x), right)
+        g_send(1, half, (gate_out, x_l), (gate_in, x), left)
+
+    def relay(half):
+        g_arrive(2, half, gate_relay, 0)
+        g_send(3, half, (gate_relay, 0), (gate_in, behind), onward)
+
     gate_in[x] = gate_out[x]
 
     w_1(0)
+    w_pass_on(1, 0)
     w_1(1)
-    o_arrive(0, x_l, 0, 128)
-    o_send(2, x_l, 0, 64, right)
-    o_arrive(1, x_r, 0, 128)
-    o_send(3, x_r, 64, 64, left)
-    for n, slot in ((4, x_l), (5, x_r)):
+    w_pass_on(0, 0)
+    o_arrive(2, x_l, 64, 64)
+    o_arrive(3, x_r, 0, 64)
+    for n, slot in ((6, x_l), (7, x_r)):
         o_send(n, slot, 0, 128, sibling)
-    w_pass_on(0, 0)
-    w_pass_on(1, 0)
-    o_arrive(2, x_a, 0, 64)
-    o_arrive(3, x_a, 64, 64)
-    o_send(6, x_a, 0, 128, sibling)
+    w_1(2)
+    w_pass_on(3, 0)
+    w_1(3)
+    w_pass_on(2, 0)
+    o_arrive(4, x_a, 0, 64)
+    o_arrive(5, x_a, 64, 64)
+    o_send(8, x_a, 0, 128, sibling)
+    relay(0)
+    relay(1)
     for n, slot in enumerate((x_l, x_r, x_a)):
-        arrive(gate_in.at[slot], ass.at[n], asr.at[n])
-    for n, slot in enumerate((x_l, x_r, x_a)):
-        arrive(ow.at[slot, pl.ds((1 - c) * 128, 128)], oss.at[4 + n], osr.at[4 + n])
-
+        arrive(ow.at[slot, pl.ds((1 - c) * 128, 128)], oss.at[6 + n], osr.at[6 + n])
     in_res.wait()
 
-    def project(n, squares):
-        cols = pl.ds(pl.multiple_of(n * 256, 256), 256)
-        acc = res[:, cols].astype(F32)
-        acc = acc + (
-            (dot(gate_in[0], ow[0, :, cols]) + dot(gate_in[1], ow[1, :, cols]))
-            + (dot(gate_in[2], ow[2, :, cols]) + dot(gate_in[3], ow[3, :, cols]))
-        )
-        stream[:, cols] = acc
-        return squares + (acc[:, :128] * acc[:, :128] + acc[:, 128:] * acc[:, 128:])
-
-    squares = lax.fori_loop(0, D // 256, project, jnp.zeros((R, 128), F32))
-    inverse = lax.rsqrt(jnp.sum(squares, axis=1, keepdims=True) / D + NORM_EPS)
-
-    def normalize(n, carry):
-        cols = pl.ds(pl.multiple_of(n * 256, 256), 256)
-        gain_row = jnp.concatenate([gsc[pl.ds(2 * n, 1), :], gsc[pl.ds(2 * n + 1, 1), :]], axis=1)
-        rows[x, :, cols] = (stream[:, cols] * inverse * gain_row).astype(BF)
-        return carry
-
-    lax.fori_loop(0, D // 256, normalize, 0)
-
-    def r_at(slot, half):
-        return rows.at[slot, pl.ds(128 * half, 128)]
-
-    def r_send(n, slot, half, device):
-        send(r_at(slot, half), r_at(slot, half), gss.at[n], gsr.at[n], device)
-
-    def r_arrive(n, slot, half):
-        arrive(r_at(slot, half), gss.at[n], gsr.at[n])
-
-    r_send(0, x, 0, right)
-    r_send(1, x, 1, left)
-    r_send(2, x, 1, right)
-    r_send(3, x, 0, left)
+    def output_rows(half):
+        span = pl.ds(128 * half, 128)
+
+        def project(n, squares):
+            cols = pl.ds(pl.multiple_of(n * 256, 256), 256)
+            cells = jnp.concatenate([gate_in[n, span] for n in range(4)], axis=1)
+            acc = res[span, cols].astype(F32) + dot(cells, ow[:, :, cols].reshape(1024, 256))
+            stream[span, cols] = acc
+            return squares + (acc[:, :128] * acc[:, :128] + acc[:, 128:] * acc[:, 128:])
+
+        squares = lax.fori_loop(0, D // 256, project, jnp.zeros((128, 128), F32))
+        inverse = lax.rsqrt(jnp.sum(squares, axis=1, keepdims=True) / D + NORM_EPS)
+
+        def normalize(n, carry):
+            cols = pl.ds(pl.multiple_of(n * 256, 256), 256)
+            gain_row = jnp.concatenate([gsc[pl.ds(2 * n, 1), :], gsc[pl.ds(2 * n + 1, 1), :]], axis=1)
+            rows[x, span, cols] = (stream[span, cols] * inverse * gain_row).astype(BF)
+            return carry
+
+        lax.fori_loop(0, D // 256, normalize, 0)
+
+    def r_at(slot, first, count):
+        return rows.at[slot, pl.ds(first, count)]
+
+    def r_send(n, slot, first, count, device):
+        send(r_at(slot, first, count), r_at(slot, first, count), gss.at[n], gsr.at[n], device)
+
+    def r_arrive(n, slot, first, count):
+        arrive(r_at(slot, first, count), gss.at[n], gsr.at[n])
+
+    def gated_rows(half):
+        for n, slot in ((0, x_l), (1, x_r), (3, x_a)):
+            g_arrive(n, half, gate_in, slot)
+
+    gated_rows(0)
+    output_rows(0)
+    r_send(0, x, 0, 128, right)
+    r_send(1, x, 0, 128, left)
+    gated_rows(1)
+    output_rows(1)
+    r_send(2, x, 128, 128, right)
+    r_send(3, x, 128, 64, left)
+    r_send(4, x, 192, 64, left)
 
     w_2(0)
     w_2(1)
@@ -506,15 +566,31 @@
         w_pass_on(1, n)
     w_finish(0, 0)
     w_finish(1, 0)
-    r_arrive(0, x_l, 0)
-    r_send(4, x_l, 0, right)
-    r_arrive(1, x_r, 1)
-    r_send(5, x_r, 1, left)
+    w_2(2)
+    w_2(3)
+    w_pass_on(1, 3)
     w_pass_on(0, 3)
-    w_pass_on(1, 3)
-    for n in (1, 2, 3):
+    for n in (1, 2):
+        w_pass_on(2, n)
+        w_pass_on(3, n)
+    r_arrive(0, x_l, 0, 128)
+    r_send(5, x_l, 0, 128, right)
+    for n in (1, 2):
         w_finish(0, n)
         w_finish(1, n)
+    w_pass_on(3, 3)
+    w_pass_on(2, 3)
+    w_finish(0, 3)
+    w_finish(1, 3)
+    for n in (0, 1, 2):
+        w_finish(2, n)
+        w_finish(3, n)
+    r_arrive(3, x_r, 128, 64)
+    r_send(6, x_r, 128, 64, left)
+    r_arrive(4, x_r, 192, 64)
+    r_send(7, x_r, 192, 64, left)
+    w_finish(2, 3)
+    w_finish(3, 3)
     for n in range(4):
         w_line(0, n, True)
         w_line(1, n, True)
@@ -564,22 +640,27 @@
         return ref.at[slot, half, pl.ds(1024 * side, 1024)]
 
     widen(0, ((x_l, up_half), (x_r, low_half)))
-    narrow(0, keep(0))
-    p_send(0, part.at[0, low_half], fin.at[0, low_half], right)
-    p_send(1, part.at[0, up_half], fin.at[1, up_half], left)
-    r_arrive(2, x_l, 1)
-    r_arrive(3, x_r, 0)
-    widen(1, ((x_r, up_half), (x_l, low_half)))
-    r_arrive(4, x_a, 0)
-    r_arrive(5, x_a, 1)
+    for n in range(4):
+        w_line(2, n, True)
+        w_line(3, n, True)
+    for side in range(2):
+        narrow(0, keep(0), 4 * side, 4 * side + 4)
+        p_send(10 * side, piece(part, 0, low_half, side), piece(fin, 0, low_half, side), right)
+        p_send(10 * side + 1, piece(part, 0, up_half, side), piece(fin, 1, up_half, side), left)
+    r_arrive(5, x_a, 0, 128)
+    r_arrive(6, x_a, 128, 64)
+    r_arrive(7, x_a, 192, 64)
     widen(2, ((x_a, up_half), (x_a, low_half)))
     for side in range(2):
         narrow(2, keep(2), 4 * side, 4 * side + 4)
         p_send(2 + 2 * side, piece(part, 2, up_half, side), piece(mid, 0, up_half, side), right)
         p_send(3 + 2 * side, piece(part, 2, low_half, side), piece(mid, 1, up_half, side), left)
+    r_arrive(2, x_l, 128, 128)
+    r_arrive(1, x_r, 0, 128)
+    widen(1, ((x_r, up_half), (x_l, low_half)))
     narrow(1, keep(1))
-    widen(3, ((x, up_half), (x, low_half)))
-    for side in range(2):
+
+    def pass_sum(side):
         at = pl.ds(1024 * side, 1024)
         p_arrive(2 + 2 * side, piece(mid, 0, up_half, side))
         part[1, up_half, at] = (part[1, up_half, at].astype(F32) + mid[0, :, at].astype(F32)).astype(BF)
@@ -587,13 +668,17 @@
         p_arrive(3 + 2 * side, piece(mid, 1, up_half, side))
         part[1, low_half, at] = (part[1, low_half, at].astype(F32) + mid[1, :, at].astype(F32)).astype(BF)
         p_send(7 + 2 * side, piece(part, 1, low_half, side), piece(fin, 1, low_half, side), left)
+
+    pass_sum(0)
+    widen(3, ((x, up_half), (x, low_half)))
+    pass_sum(1)
     def own(cols, value):
         stream[:, cols] = stream[:, cols] + 0.5 * value
 
     narrow(3, own)
-    p_arrive(0, fin.at[0, low_half])
-    p_arrive(1, fin.at[1, up_half])
     for side in range(2):
+        p_arrive(10 * side, piece(fin, 0, low_half, side))
+        p_arrive(10 * side + 1, piece(fin, 1, up_half, side))
         p_arrive(6 + 2 * side, piece(fin, 0, up_half, side))
         p_arrive(7 + 2 * side, piece(fin, 1, low_half, side))
 
@@ -628,10 +713,14 @@
     dma = pltpu.SemaphoreType.DMA
     return pl.pallas_call(
         kernel,
-        out_shape=jax.ShapeDtypeStruct((R, D), BF),
-        in_specs=[vmem] * 4 + [hbm] * 9,
+        out_shape=pltpu.VMEM((R, D), BF),
+        in_specs=[hbm] * 13,
         out_specs=vmem,
         scratch_shapes=[
+            pltpu.VMEM((2, T), F32),
+            pltpu.VMEM((2, T), F32),
+            pltpu.VMEM((8, 128), jnp.int32),
+            pltpu.VMEM((16, 128), BF),
             pltpu.VMEM((T, 256), BF),
             pltpu.VMEM((T, 256), BF),
             pltpu.VMEM((T, 256), BF),
@@ -650,6 +739,7 @@
             pltpu.VMEM((LOOK, 8, 128), F32),
             pltpu.VMEM((4, R, 256), BF),
             pltpu.VMEM((4, R, 256), BF),
+            pltpu.VMEM((1, R, 256), BF),
             pltpu.VMEM((R, D), F32),
             pltpu.VMEM((4, R, D), BF),
             pltpu.VMEM((4, R, FD), BF),
@@ -664,19 +754,19 @@
             pltpu.VMEM((2, T, 256), BF),
             pltpu.VMEM((2, T, 256), F32),
             pltpu.VMEM((T, 256), F32),
+            dma((13,)),
+            dma((4, 24)),
+            dma((4, 24)),
             dma((9,)),
-            dma((2, 24)),
-            dma((2, 24)),
-            dma((7,)),
-            dma((7,)),
-            dma((2 * LOOK + 1,)),
-            dma((2 * LOOK + 1,)),
-            dma((3,)),
-            dma((3,)),
-            dma((6,)),
-            dma((6,)),
-            dma((10,)),
-            dma((10,)),
+            dma((9,)),
+            dma((3 * LOOK + 1,)),
+            dma((3 * LOOK + 1,)),
+            dma((8,)),
+            dma((8,)),
+            dma((8,)),
+            dma((8,)),
+            dma((12,)),
+            dma((12,)),
         ],
         compiler_params=pltpu.CompilerParams(
             collective_id=0, has_side_effects=True, vmem_limit_bytes=62 * 1024 * 1024

time: 116 us -> 107 us (0.922)
  Pallas kernels: 113 us -> 106 us
  local copies, waits for them, and re-layouts: 2.3 us -> 0.97 us
    pallas_call x1, Pallas kernels: 113 us -> 106 us  [body(): pl.pallas_call(kernel, out_shape=pltpu.VMEM((R, D), BF), in_specs=[hbm] *...]
    unnamed x1, local copies, waits for them, and re-layouts: 2.3 us -> 0.97 us
where the time goes in v3:
time: 107 us
  Pallas kernels  106 us (99%)
    pallas_call x1, Pallas kernels, body(): pl.pallas_call(kernel, out_shape=pltpu.VMEM((R, D), BF), in_specs=[hbm] *...  106 us

profile of v3, /device:TPU:1, one launch (start us, length us, event | category | flops | bytes accessed | tf_op | source)
XLA Modules:
  0.0 107.3 jit_solution(14115811673033654363)
XLA Ops:
  0.0 106.3 %shard_map.127 = bf16[256,2048]{1,0:T(8,128)(2,1)S(1)} custom-call(f32[2,1024]{1,0:T(2,128)} %in_gate_hbm.1, f32[2,1024]{1,0:T(2,128)} %forget_hbm.1, s32[8,128]{1,0:T(8,128)} %bitcast.4, bf16[16,128]{1,0:T(8,128)(2,1)} %bitcast.5, bf16[1024,256]{1,0:T(8,128)(2,1)} %q_hbm.1, bf16[1024,256]{1,0:T(8,128)(2,1)} %k_hbm.1, bf16[1024,256]{1,0:T(8,128)(2,1)} %v_hbm.1, ...), custom_call_target="tpu_custom_call" | custom-call | tf_op jit(solution)/shard_map/pallas_call | solution.py:714
  106.3 1.0 copy.15

commit v4 on v3

--- a/solution.py
+++ b/solution.py
@@ -154,8 +154,6 @@
         local.append(copy)
     small, (in_ow, in_wg, in_wu, in_wd, in_k, in_v, in_q, in_og, in_res) = local[:4], local[4:]
 
-    sent = []
-
     def remote(src, dst, send_sem, recv_sem, device):
         return pltpu.make_async_remote_copy(
             src_ref=src,
@@ -167,9 +165,10 @@
         )
 
     def send(*args):
-        copy = remote(*args)
-        copy.start()
-        sent.append(copy)
+        remote(*args).start()
+
+    def drain(ref, sem):
+        remote(ref, ref, sem, lsem.at[0], sibling).wait_send()
 
     def arrive(ref, send_sem, recv_sem):
         remote(ref, ref, send_sem, recv_sem, sibling).wait_recv()
@@ -183,10 +182,13 @@
 
     def w_send(p, n, first, count, uu, vv, device):
         ref = w_at(p, first, count, uu, vv)
-        send(ref, ref, wss.at[p, n], wsr.at[p, n], device)
-
-    def w_arrive(p, n, first, count, uu, vv):
-        arrive(w_at(p, first, count, uu, vv), wss.at[p, n], wsr.at[p, n])
+        place = (0, 1, 2, 2)[n] if n < 4 else 3 * (n // 4) + (0, 1, 2, 2)[n % 4]
+        group = 2 * (n // 4 > 0) + (n % 4 > 1)
+        send(ref, ref, wss.at[group], wsr.at[p, place], device)
+
+    def w_arrive(p, place, uu, vv):
+        first, count, _ = PARTS[p]
+        arrive(w_at(p, first, count, uu, vv), wss.at[0], wsr.at[p, place])
 
     LINE = (0, -1, 1, 2)
 
@@ -200,30 +202,27 @@
         (_, uu), (vn, vv) = w_axes(p)
         first, count, half = PARTS[p]
         k_at = step(uu, LINE[n])
-        w_arrive(p, 4 + 4 * n, first, count, k_at, step(vv, -1))
+        w_arrive(p, 3 + 3 * n, k_at, step(vv, -1))
         w_send(p, 6 + 4 * n, first, half, k_at, step(vv, -1), {vn: step(vv, 1)})
-        w_arrive(p, 5 + 4 * n, first, count, k_at, step(vv, 1))
+        w_arrive(p, 4 + 3 * n, k_at, step(vv, 1))
         w_send(p, 7 + 4 * n, first + half, count - half, k_at, step(vv, 1), {vn: step(vv, -1)})
 
-    def w_line(p, n, get):
+    def w_line(p, n):
         (_, uu), _ = w_axes(p)
         first, count, _ = PARTS[p]
         k_at = step(uu, LINE[n])
-        core = 1 - c if get else c
         span = pl.ds(first, count)
-        ref = w.at[span, k_at, :, core] if p % 2 == 0 else w.at[span, :, k_at, core]
-        if get:
-            arrive(ref, wss.at[p, 20 + n], wsr.at[p, 20 + n])
-        else:
-            send(ref, ref, wss.at[p, 20 + n], wsr.at[p, 20 + n], sibling)
+        ref = w.at[span, k_at, :, c] if p % 2 == 0 else w.at[span, :, k_at, c]
+        send(ref, ref, wss.at[4 + p // 2], wsr.at[0, 15 + p // 2], sibling)
+
+    def w_twin(kind):
+        first, count = ((0, 2 * NJ), (2 * NJ, NJ))[kind]
+        arrive(w.at[pl.ds(first, count), :, :, 1 - c], wss.at[0], wsr.at[0, 15 + kind])
 
     def w_finish(p, n):
         (_, uu), (_, vv) = w_axes(p)
-        first, count, half = PARTS[p]
-        k_at = step(uu, LINE[n])
-        w_arrive(p, 6 + 4 * n, first, half, k_at, step(vv, 2))
-        w_arrive(p, 7 + 4 * n, first + half, count - half, k_at, step(vv, 2))
-        w_line(p, n, False)
+        w_arrive(p, 5 + 3 * n, step(uu, LINE[n]), step(vv, 2))
+        w_line(p, n)
 
     def w_0(name):
         for p in (0, 1, 2, 3) if name == "sp_0" else (1, 0, 3, 2):
@@ -238,18 +237,16 @@
     def w_1(p):
         (un, uu), (_, vv) = w_axes(p)
         first, count, half = PARTS[p]
-        w_arrive(p, 0, first, count, step(uu, -1), vv)
+        w_arrive(p, 0, step(uu, -1), vv)
         w_send(p, 2, first, half, step(uu, -1), vv, {un: step(uu, 1)})
         w_spread(p, 1)
-        w_arrive(p, 1, first, count, step(uu, 1), vv)
+        w_arrive(p, 1, step(uu, 1), vv)
         w_send(p, 3, first + half, count - half, step(uu, 1), vv, {un: step(uu, -1)})
         w_spread(p, 2)
 
     def w_2(p):
         (_, uu), (_, vv) = w_axes(p)
-        first, count, half = PARTS[p]
-        w_arrive(p, 2, first, half, step(uu, 2), vv)
-        w_arrive(p, 3, first + half, count - half, step(uu, 2), vv)
+        w_arrive(p, 2, step(uu, 2), vv)
         w_spread(p, 3)
 
     right, left, across = {"tp": step(x, 1)}, {"tp": step(x, -1)}, {"tp": step(x, 2)}
@@ -259,18 +256,18 @@
         return ow.at[slot, pl.ds(c * 128 + part_first, count)]
 
     def o_send(n, slot, first, count, device):
-        send(o_at(slot, first, count), o_at(slot, first, count), oss.at[n], osr.at[n], device)
+        send(o_at(slot, first, count), o_at(slot, first, count), oss, osr.at[n], device)
 
 
     def o_arrive(n, slot, first, count):
-        arrive(o_at(slot, first, count), oss.at[n], osr.at[n])
+        arrive(o_at(slot, first, count), oss, osr.at[n])
 
     pl.semaphore_wait(barrier, len(peers))
     in_ow.wait()
     o_send(0, x, 0, 64, right)
     o_send(1, x, 64, 64, left)
     o_send(2, x, 64, 64, right)
-    o_send(3, x, 0, 64, left)
+    o_send(2, x, 0, 64, left)
 
     in_wg.wait()
     in_wu.wait()
@@ -376,8 +373,8 @@
     meta_out[...] = jnp.concatenate(meta, axis=0)
     head = pl.ds(HD * c, HD)
     for d in range(1, LOOK + 1):
-        send(meta_out, meta_in.at[d - 1], sss.at[2 * d], ssr.at[2 * d], chip_ahead(d))
-        send(mem_out.at[head], mem_in.at[d - 1, head], sss.at[2 * d - 1], ssr.at[2 * d - 1], chip_ahead(d))
+        send(meta_out, meta_in.at[d - 1], sss.at[1], ssr.at[1], chip_ahead(d))
+        send(mem_out.at[head], mem_in.at[d - 1, head], sss.at[2], ssr.at[2], chip_ahead(d))
 
     w_0("sp_1")
 
@@ -417,17 +414,14 @@
         opened[at, :] = 1.0 / (1.0 + jnp.exp(-og[at, :].astype(F32)))
 
     o_arrive(0, x_l, 0, 64)
-    o_send(4, x_l, 0, 64, right)
+    o_send(3, x_l, 0, 64, right)
     o_arrive(1, x_r, 64, 64)
-    o_send(5, x_r, 64, 64, left)
-    for d in range(1, LOOK + 1):
-        arrive(mem_in.at[d - 1, head], sss.at[2 * d - 1], ssr.at[2 * d - 1])
-        n = 2 * LOOK + d
-        send(mem_in.at[d - 1, head], mem_in.at[d - 1, head], sss.at[n], ssr.at[n], sibling)
-    for d in range(1, LOOK + 1):
-        n = 2 * LOOK + d
-        arrive(meta_in.at[d - 1], sss.at[2 * d], ssr.at[2 * d])
-        arrive(mem_in.at[d - 1, pl.ds(HD * (1 - c), HD)], sss.at[n], ssr.at[n])
+    o_send(3, x_r, 64, 64, left)
+    arrive(mem_in.at[:, head], sss.at[2], ssr.at[2])
+    for d in range(LOOK):
+        send(mem_in.at[d, head], mem_in.at[d, head], sss.at[2], ssr.at[3], sibling)
+    arrive(meta_in, sss.at[1], ssr.at[1])
+    arrive(mem_in.at[:, pl.ds(HD * (1 - c), HD)], sss.at[2], ssr.at[3])
     second_core = c == 1
     one_back = meta_in[0, 6:7, :]
     carry_doc = jnp.where(second_core, twin[6:7, :], jnp.where(chip > 0, one_back, -1.0))
@@ -475,22 +469,17 @@
     onward, behind = {"tp": lax.rem(x + 1 + 2 * c, 4)}, lax.rem(x + 3 + 2 * c, 4)
 
     def g_send(n, half, src, dst, device):
-        m = 4 * half + n
-        send(half_of(*src, half), half_of(*dst, half), ass.at[m], asr.at[m], device)
-
-    def g_arrive(n, half, ref, slot):
-        m = 4 * half + n
-        arrive(half_of(ref, slot, half), ass.at[m], asr.at[m])
+        send(half_of(*src, half), half_of(*dst, half), ass, asr.at[2 * n + half], device)
 
     for half in range(2):
-        g_send(2, half, (gate_out, x_a), (gate_relay, 0), onward)
+        g_send(0, half, (gate_out, x_a), (gate_relay, 0), onward)
     for half in range(2):
-        g_send(0, half, (gate_out, x_r), (gate_in, x), right)
+        g_send(1, half, (gate_out, x_r), (gate_in, x), right)
         g_send(1, half, (gate_out, x_l), (gate_in, x), left)
 
     def relay(half):
-        g_arrive(2, half, gate_relay, 0)
-        g_send(3, half, (gate_relay, 0), (gate_in, behind), onward)
+        arrive(half_of(gate_relay, 0, half), ass, asr.at[half])
+        g_send(1, half, (gate_relay, 0), (gate_in, behind), onward)
 
     gate_in[x] = gate_out[x]
 
@@ -498,21 +487,18 @@
     w_pass_on(1, 0)
     w_1(1)
     w_pass_on(0, 0)
-    o_arrive(2, x_l, 64, 64)
-    o_arrive(3, x_r, 0, 64)
-    for n, slot in ((6, x_l), (7, x_r)):
-        o_send(n, slot, 0, 128, sibling)
+    o_arrive(2, x_l, 0, 128)
+    for slot in (x_l, x_r):
+        o_send(4, slot, 0, 128, sibling)
     w_1(2)
     w_pass_on(3, 0)
     w_1(3)
     w_pass_on(2, 0)
-    o_arrive(4, x_a, 0, 64)
-    o_arrive(5, x_a, 64, 64)
-    o_send(8, x_a, 0, 128, sibling)
+    o_arrive(3, x_a, 0, 128)
+    o_send(4, x_a, 0, 128, sibling)
     relay(0)
     relay(1)
-    for n, slot in enumerate((x_l, x_r, x_a)):
-        arrive(ow.at[slot, pl.ds((1 - c) * 128, 128)], oss.at[6 + n], osr.at[6 + n])
+    arrive(ow.at[pl.ds(0, 3), pl.ds((1 - c) * 128, 128)], oss, osr.at[4])
     in_res.wait()
 
     def output_rows(half):
@@ -540,14 +526,13 @@
         return rows.at[slot, pl.ds(first, count)]
 
     def r_send(n, slot, first, count, device):
-        send(r_at(slot, first, count), r_at(slot, first, count), gss.at[n], gsr.at[n], device)
+        send(r_at(slot, first, count), r_at(slot, first, count), gss, gsr.at[n], device)
 
     def r_arrive(n, slot, first, count):
-        arrive(r_at(slot, first, count), gss.at[n], gsr.at[n])
+        arrive(r_at(slot, first, count), gss, gsr.at[n])
 
     def gated_rows(half):
-        for n, slot in ((0, x_l), (1, x_r), (3, x_a)):
-            g_arrive(n, half, gate_in, slot)
+        arrive(gate_in.at[pl.ds(0, 3), pl.ds(128 * half, 128)], ass, asr.at[2 + half])
 
     gated_rows(0)
     output_rows(0)
@@ -555,9 +540,9 @@
     r_send(1, x, 0, 128, left)
     gated_rows(1)
     output_rows(1)
-    r_send(2, x, 128, 128, right)
-    r_send(3, x, 128, 64, left)
-    r_send(4, x, 192, 64, left)
+    r_send(1, x, 128, 128, right)
+    r_send(2, x, 128, 64, left)
+    r_send(3, x, 192, 64, left)
 
     w_2(0)
     w_2(1)
@@ -574,7 +559,7 @@
         w_pass_on(2, n)
         w_pass_on(3, n)
     r_arrive(0, x_l, 0, 128)
-    r_send(5, x_l, 0, 128, right)
+    r_send(4, x_l, 0, 128, right)
     for n in (1, 2):
         w_finish(0, n)
         w_finish(1, n)
@@ -585,15 +570,13 @@
     for n in (0, 1, 2):
         w_finish(2, n)
         w_finish(3, n)
-    r_arrive(3, x_r, 128, 64)
-    r_send(6, x_r, 128, 64, left)
-    r_arrive(4, x_r, 192, 64)
-    r_send(7, x_r, 192, 64, left)
+    r_arrive(2, x_r, 128, 64)
+    r_send(4, x_r, 128, 64, left)
+    r_arrive(3, x_r, 192, 64)
+    r_send(4, x_r, 192, 64, left)
     w_finish(2, 3)
     w_finish(3, 3)
-    for n in range(4):
-        w_line(0, n, True)
-        w_line(1, n, True)
+    w_twin(0)
 
     up_half, low_half = pl.ds(0, 128), pl.ds(128, 128)
 
@@ -631,43 +614,37 @@
         return store
 
     def p_send(n, src, dst, device):
-        send(src, dst, rss.at[n], rsr.at[n], device)
+        send(src, dst, rss, rsr.at[n], device)
 
     def p_arrive(n, ref):
-        arrive(ref, rss.at[n], rsr.at[n])
+        arrive(ref, rss, rsr.at[n])
 
     def piece(ref, slot, half, side):
         return ref.at[slot, half, pl.ds(1024 * side, 1024)]
 
     widen(0, ((x_l, up_half), (x_r, low_half)))
-    for n in range(4):
-        w_line(2, n, True)
-        w_line(3, n, True)
+    w_twin(1)
     for side in range(2):
         narrow(0, keep(0), 4 * side, 4 * side + 4)
-        p_send(10 * side, piece(part, 0, low_half, side), piece(fin, 0, low_half, side), right)
-        p_send(10 * side + 1, piece(part, 0, up_half, side), piece(fin, 1, up_half, side), left)
-    r_arrive(5, x_a, 0, 128)
-    r_arrive(6, x_a, 128, 64)
-    r_arrive(7, x_a, 192, 64)
+        p_send(side, piece(part, 0, low_half, side), piece(fin, 0, low_half, side), right)
+        p_send(side, piece(part, 0, up_half, side), piece(fin, 1, up_half, side), left)
+    r_arrive(4, x_a, 0, R)
     widen(2, ((x_a, up_half), (x_a, low_half)))
     for side in range(2):
         narrow(2, keep(2), 4 * side, 4 * side + 4)
-        p_send(2 + 2 * side, piece(part, 2, up_half, side), piece(mid, 0, up_half, side), right)
-        p_send(3 + 2 * side, piece(part, 2, low_half, side), piece(mid, 1, up_half, side), left)
-    r_arrive(2, x_l, 128, 128)
-    r_arrive(1, x_r, 0, 128)
+        p_send(2 + side, piece(part, 2, up_half, side), piece(mid, 0, up_half, side), right)
+        p_send(2 + side, piece(part, 2, low_half, side), piece(mid, 1, up_half, side), left)
+    r_arrive(1, x_r, 0, R)
     widen(1, ((x_r, up_half), (x_l, low_half)))
     narrow(1, keep(1))
 
     def pass_sum(side):
         at = pl.ds(1024 * side, 1024)
-        p_arrive(2 + 2 * side, piece(mid, 0, up_half, side))
+        p_arrive(2 + side, mid.at[:, :, at])
         part[1, up_half, at] = (part[1, up_half, at].astype(F32) + mid[0, :, at].astype(F32)).astype(BF)
-        p_send(6 + 2 * side, piece(part, 1, up_half, side), piece(fin, 0, up_half, side), right)
-        p_arrive(3 + 2 * side, piece(mid, 1, up_half, side))
+        p_send(side, piece(part, 1, up_half, side), piece(fin, 0, up_half, side), right)
         part[1, low_half, at] = (part[1, low_half, at].astype(F32) + mid[1, :, at].astype(F32)).astype(BF)
-        p_send(7 + 2 * side, piece(part, 1, low_half, side), piece(fin, 1, low_half, side), left)
+        p_send(side, piece(part, 1, low_half, side), piece(fin, 1, low_half, side), left)
 
     pass_sum(0)
     widen(3, ((x, up_half), (x, low_half)))
@@ -677,20 +654,30 @@
 
     narrow(3, own)
     for side in range(2):
-        p_arrive(10 * side, piece(fin, 0, low_half, side))
-        p_arrive(10 * side + 1, piece(fin, 1, up_half, side))
-        p_arrive(6 + 2 * side, piece(fin, 0, up_half, side))
-        p_arrive(7 + 2 * side, piece(fin, 1, low_half, side))
-
-    def finish(n, carry):
-        cols = pl.ds(pl.multiple_of(n * 256, 256), 256)
-        others = fin[0, :, cols].astype(F32) + fin[1, :, cols].astype(F32)
-        out[:, cols] = (stream[:, cols] + 0.5 * others).astype(BF)
-        return carry
-
-    lax.fori_loop(0, D // 256, finish, 0)
-    for copy in sent:
-        copy.wait_send()
+        at = pl.ds(1024 * side, 1024)
+        p_arrive(side, fin.at[:, :, at])
+
+        def finish(n, carry):
+            cols = pl.ds(pl.multiple_of(n * 256, 256), 256)
+            others = fin[0, :, cols].astype(F32) + fin[1, :, cols].astype(F32)
+            out[:, cols] = (stream[:, cols] + 0.5 * others).astype(BF)
+            return carry
+
+        lax.fori_loop(4 * side, 4 * side + 4, finish, 0)
+
+    drain(w.at[:, pl.ds(0, 1), pl.ds(0, 1)], wss.at[0])
+    drain(w.at[:, pl.ds(0, 1), pl.ds(0, 1), pl.ds(0, 1)], wss.at[1])
+    drain(w.at[:, pl.ds(0, 1)], wss.at[2])
+    drain(w.at[:, pl.ds(0, 1), :, pl.ds(0, 1)], wss.at[3])
+    drain(w.at[pl.ds(0, 2 * NJ), :, :, pl.ds(0, 1)], wss.at[4])
+    drain(w.at[pl.ds(0, NJ), :, :, pl.ds(0, 1)], wss.at[5])
+    drain(ow.at[pl.ds(0, 3)], oss)
+    drain(st_out, sss.at[0])
+    drain(meta_in, sss.at[1])
+    drain(mem_in, sss.at[2])
+    drain(gate_in, ass)
+    drain(rows.at[pl.ds(0, 3)], gss)
+    drain(part, rss)
 
 
 def body(
@@ -755,18 +742,18 @@
             pltpu.VMEM((2, T, 256), F32),
             pltpu.VMEM((T, 256), F32),
             dma((13,)),
-            dma((4, 24)),
-            dma((4, 24)),
-            dma((9,)),
-            dma((9,)),
-            dma((3 * LOOK + 1,)),
-            dma((3 * LOOK + 1,)),
-            dma((8,)),
-            dma((8,)),
-            dma((8,)),
-            dma((8,)),
-            dma((12,)),
-            dma((12,)),
+            dma((6,)),
+            dma((4, 17)),
+            dma(()),
+            dma((5,)),
+            dma((3,)),
+            dma((4,)),
+            dma(()),
+            dma((4,)),
+            dma(()),
+            dma((5,)),
+            dma(()),
+            dma((4,)),
         ],
         compiler_params=pltpu.CompilerParams(
             collective_id=0, has_side_effects=True, vmem_limit_bytes=62 * 1024 * 1024

time: 107 us -> 105 us (0.981)
  Pallas kernels: 106 us -> 104 us
    pallas_call x1, Pallas kernels: 106 us -> 104 us  [body(): pl.pallas_call(kernel, out_shape=pltpu.VMEM((R, D), BF), in_specs=[hbm] *...]
where the time goes in v4:
time: 105 us
  Pallas kernels  104 us (99%)
    pallas_call x1, Pallas kernels, body(): pl.pallas_call(kernel, out_shape=pltpu.VMEM((R, D), BF), in_specs=[hbm] *...  104 us

profile of v4, /device:TPU:1, one launch (start us, length us, event | category | flops | bytes accessed | tf_op | source)
XLA Modules:
  0.0 105.2 jit_solution(9167183043471654682)
XLA Ops:
  0.0 104.2 %shard_map.127 = bf16[256,2048]{1,0:T(8,128)(2,1)S(1)} custom-call(f32[2,1024]{1,0:T(2,128)} %in_gate_hbm.1, f32[2,1024]{1,0:T(2,128)} %forget_hbm.1, s32[8,128]{1,0:T(8,128)} %bitcast.4, bf16[16,128]{1,0:T(8,128)(2,1)} %bitcast.5, bf16[1024,256]{1,0:T(8,128)(2,1)} %q_hbm.1, bf16[1024,256]{1,0:T(8,128)(2,1)} %k_hbm.1, bf16[1024,256]{1,0:T(8,128)(2,1)} %v_hbm.1, ...), custom_call_target="tpu_custom_call" | custom-call | tf_op jit(solution)/shard_map/pallas_call | solution.py:701
  104.2 1.0 copy.15

commit v5 on v4

--- a/solution.py
+++ b/solution.py
@@ -94,6 +94,8 @@
     vones,
     numden,
     opened,
+    inverses,
+    factor,
     lsem,
     wss,
     wsr,
@@ -105,6 +107,8 @@
     asr,
     gss,
     gsr,
+    iss,
+    isr,
     rss,
     rsr,
 ):
@@ -206,13 +210,13 @@
         w_send(p, 6 + 4 * n, first, half, k_at, step(vv, -1), {vn: step(vv, 1)})
         w_arrive(p, 4 + 3 * n, k_at, step(vv, 1))
         w_send(p, 7 + 4 * n, first + half, count - half, k_at, step(vv, 1), {vn: step(vv, -1)})
-
-    def w_line(p, n):
-        (_, uu), _ = w_axes(p)
+        for by in (0, -1, 1) if p < 2 else ():
+            w_hand_over(p, n, by)
+
+    def w_hand_over(p, n, by):
+        (_, uu), (_, vv) = w_axes(p)
         first, count, _ = PARTS[p]
-        k_at = step(uu, LINE[n])
-        span = pl.ds(first, count)
-        ref = w.at[span, k_at, :, c] if p % 2 == 0 else w.at[span, :, k_at, c]
+        ref = w_at(p, first, count, step(uu, LINE[n]), step(vv, by))
         send(ref, ref, wss.at[4 + p // 2], wsr.at[0, 15 + p // 2], sibling)
 
     def w_twin(kind):
@@ -222,7 +226,8 @@
     def w_finish(p, n):
         (_, uu), (_, vv) = w_axes(p)
         w_arrive(p, 5 + 3 * n, step(uu, LINE[n]), step(vv, 2))
-        w_line(p, n)
+        for by in (2,) if p < 2 else (0, -1, 1, 2):
+            w_hand_over(p, n, by)
 
     def w_0(name):
         for p in (0, 1, 2, 3) if name == "sp_0" else (1, 0, 3, 2):
@@ -471,11 +476,12 @@
     def g_send(n, half, src, dst, device):
         send(half_of(*src, half), half_of(*dst, half), ass, asr.at[2 * n + half], device)
 
-    for half in range(2):
+    def g_start(half):
         g_send(0, half, (gate_out, x_a), (gate_relay, 0), onward)
-    for half in range(2):
         g_send(1, half, (gate_out, x_r), (gate_in, x), right)
         g_send(1, half, (gate_out, x_l), (gate_in, x), left)
+
+    g_start(0)
 
     def relay(half):
         arrive(half_of(gate_relay, 0, half), ass, asr.at[half])
@@ -497,52 +503,52 @@
     o_arrive(3, x_a, 0, 128)
     o_send(4, x_a, 0, 128, sibling)
     relay(0)
-    relay(1)
+    g_start(1)
     arrive(ow.at[pl.ds(0, 3), pl.ds((1 - c) * 128, 128)], oss, osr.at[4])
     in_res.wait()
 
-    def output_rows(half):
+    def r_at(slot, first, count):
+        return rows.at[slot, pl.ds(first, count)]
+
+    def r_send(n, slot, first, count, device):
+        send(r_at(slot, first, count), r_at(slot, first, count), gss, gsr.at[n], device)
+
+    def r_arrive(n, slot, first, count):
+        arrive(r_at(slot, first, count), gss, gsr.at[n])
+
+    def output_rows(half, devices):
         span = pl.ds(128 * half, 128)
+        cells = jnp.concatenate([gate_in[n, span] for n in range(4)], axis=1)
 
         def project(n, squares):
             cols = pl.ds(pl.multiple_of(n * 256, 256), 256)
-            cells = jnp.concatenate([gate_in[n, span] for n in range(4)], axis=1)
             acc = res[span, cols].astype(F32) + dot(cells, ow[:, :, cols].reshape(1024, 256))
             stream[span, cols] = acc
+            gain_row = jnp.concatenate([gsc[pl.ds(2 * n, 1), :], gsc[pl.ds(2 * n + 1, 1), :]], axis=1)
+            rows[x, span, cols] = (acc * gain_row).astype(BF)
             return squares + (acc[:, :128] * acc[:, :128] + acc[:, 128:] * acc[:, 128:])
 
-        squares = lax.fori_loop(0, D // 256, project, jnp.zeros((128, 128), F32))
+        squares = jnp.zeros((128, 128), F32)
+        for part_of in range(4):
+            squares = lax.fori_loop(2 * part_of, 2 * part_of + 2, project, squares)
+            cols = pl.ds(512 * part_of, 512)
+            for n, first, count, device in devices:
+                ref = rows.at[x, pl.ds(128 * half + first, count), cols]
+                send(ref, ref, gss, gsr.at[n], device)
         inverse = lax.rsqrt(jnp.sum(squares, axis=1, keepdims=True) / D + NORM_EPS)
-
-        def normalize(n, carry):
-            cols = pl.ds(pl.multiple_of(n * 256, 256), 256)
-            gain_row = jnp.concatenate([gsc[pl.ds(2 * n, 1), :], gsc[pl.ds(2 * n + 1, 1), :]], axis=1)
-            rows[x, span, cols] = (stream[span, cols] * inverse * gain_row).astype(BF)
-            return carry
-
-        lax.fori_loop(0, D // 256, normalize, 0)
-
-    def r_at(slot, first, count):
-        return rows.at[slot, pl.ds(first, count)]
-
-    def r_send(n, slot, first, count, device):
-        send(r_at(slot, first, count), r_at(slot, first, count), gss, gsr.at[n], device)
-
-    def r_arrive(n, slot, first, count):
-        arrive(r_at(slot, first, count), gss, gsr.at[n])
+        at = pl.ds(8 * half, 8)
+        inverses[x, at] = jnp.broadcast_to(inverse, (128, 128)).T[0:8, :]
+        for device in (right, left, across):
+            send(inverses.at[x, at], inverses.at[x, at], iss, isr, device)
 
     def gated_rows(half):
         arrive(gate_in.at[pl.ds(0, 3), pl.ds(128 * half, 128)], ass, asr.at[2 + half])
 
     gated_rows(0)
-    output_rows(0)
-    r_send(0, x, 0, 128, right)
-    r_send(1, x, 0, 128, left)
+    relay(1)
+    output_rows(0, ((0, 0, 128, right), (1, 0, 128, left)))
     gated_rows(1)
-    output_rows(1)
-    r_send(1, x, 128, 128, right)
-    r_send(2, x, 128, 64, left)
-    r_send(3, x, 192, 64, left)
+    output_rows(1, ((1, 0, 128, right), (2, 0, 64, left), (3, 64, 64, left)))
 
     w_2(0)
     w_2(1)
@@ -567,31 +573,34 @@
     w_pass_on(2, 3)
     w_finish(0, 3)
     w_finish(1, 3)
-    for n in (0, 1, 2):
+    r_arrive(2, x_r, 128, 64)
+    r_send(4, x_r, 128, 64, left)
+    for n in range(3):
         w_finish(2, n)
         w_finish(3, n)
-    r_arrive(2, x_r, 128, 64)
-    r_send(4, x_r, 128, 64, left)
     r_arrive(3, x_r, 192, 64)
     r_send(4, x_r, 192, 64, left)
-    w_finish(2, 3)
-    w_finish(3, 3)
     w_twin(0)
 
+    arrive(inverses.at[pl.ds(0, 3)], iss, isr)
     up_half, low_half = pl.ds(0, 128), pl.ds(128, 128)
 
-    def widen(n, pieces):
+    def widen(n, pieces, first=0, last=NJ):
+        for m, (slot, half) in enumerate(pieces):
+            row_of = inverses[slot, pl.ds(half.start // 16, 8)][0:1, :]
+            factor[128 * m : 128 * m + 128, :] = jnp.broadcast_to(row_of, (128, 128)).T
+
         def one(j, carry):
             both = jnp.concatenate(
                 [w[2 * j].reshape(D, 128), w[2 * j + 1].reshape(D, 128)], axis=1
             )
             acts = dot(jnp.concatenate([rows[piece] for piece in pieces], axis=0), both)
-            gate_act, up_act = acts[:, :128], acts[:, 128:]
+            gate_act, up_act = acts[:, :128] * factor[...], acts[:, 128:] * factor[...]
             cols = pl.ds(pl.multiple_of(j * 128, 128), 128)
             hid[n, :, cols] = (gate_act * (1.0 / (1.0 + jnp.exp(-gate_act))) * up_act).astype(BF)
             return carry
 
-        lax.fori_loop(0, NJ, one, 0)
+        lax.fori_loop(first, last, one, 0)
 
     def narrow(n, store, first=0, last=D // 256):
         def one(t, carry):
@@ -622,12 +631,17 @@
     def piece(ref, slot, half, side):
         return ref.at[slot, half, pl.ds(1024 * side, 1024)]
 
-    widen(0, ((x_l, up_half), (x_r, low_half)))
+    pieces = ((x_l, up_half), (x_r, low_half))
+    widen(0, pieces, 0, 6)
+    w_finish(2, 3)
+    w_finish(3, 3)
+    widen(0, pieces, 6, NJ)
     w_twin(1)
-    for side in range(2):
-        narrow(0, keep(0), 4 * side, 4 * side + 4)
-        p_send(side, piece(part, 0, low_half, side), piece(fin, 0, low_half, side), right)
-        p_send(side, piece(part, 0, up_half, side), piece(fin, 1, up_half, side), left)
+    for t in range(4):
+        narrow(0, keep(0), 2 * t, 2 * t + 2)
+        at = pl.ds(512 * t, 512)
+        p_send(t // 2, part.at[0, low_half, at], fin.at[0, low_half, at], right)
+        p_send(t // 2, part.at[0, up_half, at], fin.at[1, up_half, at], left)
     r_arrive(4, x_a, 0, R)
     widen(2, ((x_a, up_half), (x_a, low_half)))
     for side in range(2):
@@ -677,6 +691,7 @@
     drain(mem_in, sss.at[2])
     drain(gate_in, ass)
     drain(rows.at[pl.ds(0, 3)], gss)
+    drain(inverses.at[pl.ds(0, 3)], iss)
     drain(part, rss)
 
 
@@ -741,6 +756,8 @@
             pltpu.VMEM((2, T, 256), BF),
             pltpu.VMEM((2, T, 256), F32),
             pltpu.VMEM((T, 256), F32),
+            pltpu.VMEM((4, 16, 128), F32),
+            pltpu.VMEM((R, 128), F32),
             dma((13,)),
             dma((6,)),
             dma((4, 17)),
@@ -752,6 +769,8 @@
             dma((4,)),
             dma(()),
             dma((5,)),
+            dma(()),
+            dma(()),
             dma(()),
             dma((4,)),
         ],

time: 105 us -> 104 us (level)
    pallas_call x1, Pallas kernels: 104 us -> 103 us  [body(): pl.pallas_call(kernel, out_shape=pltpu.VMEM((R, D), BF), in_specs=[hbm] *...]
where the time goes in v5:
time: 104 us
  Pallas kernels  103 us (99%)
    pallas_call x1, Pallas kernels, body(): pl.pallas_call(kernel, out_shape=pltpu.VMEM((R, D), BF), in_specs=[hbm] *...  103 us

profile of v5, /device:TPU:1, one launch (start us, length us, event | category | flops | bytes accessed | tf_op | source)
XLA Modules:
  0.0 103.5 jit_solution(3636309407535553475)
XLA Ops:
  0.0 102.6 %shard_map.127 = bf16[256,2048]{1,0:T(8,128)(2,1)S(1)} custom-call(f32[2,1024]{1,0:T(2,128)} %in_gate_hbm.1, f32[2,1024]{1,0:T(2,128)} %forget_hbm.1, s32[8,128]{1,0:T(8,128)} %bitcast.4, bf16[16,128]{1,0:T(8,128)(2,1)} %bitcast.5, bf16[1024,256]{1,0:T(8,128)(2,1)} %q_hbm.1, bf16[1024,256]{1,0:T(8,128)(2,1)} %k_hbm.1, bf16[1024,256]{1,0:T(8,128)(2,1)} %v_hbm.1, ...), custom_call_target="tpu_custom_call" | custom-call | tf_op jit(solution)/shard_map/pallas_call | solution.py:716
  102.6 1.0 copy.15

commit v6 on v5

--- a/solution.py
+++ b/solution.py
@@ -421,7 +421,7 @@
     o_arrive(0, x_l, 0, 64)
     o_send(3, x_l, 0, 64, right)
     o_arrive(1, x_r, 64, 64)
-    o_send(3, x_r, 64, 64, left)
+    o_send(5, x_r, 64, 64, left)
     arrive(mem_in.at[:, head], sss.at[2], ssr.at[2])
     for d in range(LOOK):
         send(mem_in.at[d, head], mem_in.at[d, head], sss.at[2], ssr.at[3], sibling)
@@ -500,8 +500,10 @@
     w_pass_on(3, 0)
     w_1(3)
     w_pass_on(2, 0)
-    o_arrive(3, x_a, 0, 128)
-    o_send(4, x_a, 0, 128, sibling)
+    o_arrive(3, x_a, 0, 64)
+    o_send(4, x_a, 0, 64, sibling)
+    o_arrive(5, x_a, 64, 64)
+    o_send(4, x_a, 64, 64, sibling)
     relay(0)
     g_start(1)
     arrive(ow.at[pl.ds(0, 3), pl.ds((1 - c) * 128, 128)], oss, osr.at[4])
@@ -762,7 +764,7 @@
             dma((6,)),
             dma((4, 17)),
             dma(()),
-            dma((5,)),
+            dma((6,)),
             dma((3,)),
             dma((4,)),
             dma(()),

time: 104 us -> 104 us (level)
  no operation moved by 1% of the time
where the time goes in v6:
time: 104 us
  Pallas kernels  103 us (99%)
    pallas_call x1, Pallas kernels, body(): pl.pallas_call(kernel, out_shape=pltpu.VMEM((R, D), BF), in_specs=[hbm] *...  103 us

profile of v6, /device:TPU:1, one launch (start us, length us, event | category | flops | bytes accessed | tf_op | source)
XLA Modules:
  0.0 103.5 jit_solution(14069346743131096357)
XLA Ops:
  0.0 102.6 %shard_map.127 = bf16[256,2048]{1,0:T(8,128)(2,1)S(1)} custom-call(f32[2,1024]{1,0:T(2,128)} %in_gate_hbm.1, f32[2,1024]{1,0:T(2,128)} %forget_hbm.1, s32[8,128]{1,0:T(8,128)} %bitcast.4, bf16[16,128]{1,0:T(8,128)(2,1)} %bitcast.5, bf16[1024,256]{1,0:T(8,128)(2,1)} %q_hbm.1, bf16[1024,256]{1,0:T(8,128)(2,1)} %k_hbm.1, bf16[1024,256]{1,0:T(8,128)(2,1)} %v_hbm.1, ...), custom_call_target="tpu_custom_call" | custom-call | tf_op jit(solution)/shard_map/pallas_call | solution.py:718
  102.6 1.0 copy.15
